TPU v7x, 128 devices: a whole 4x4x4 slice. The times are simulated.
128 devices in a mesh: kv: 16 (over z, x), tp: 8 (over y, core).
Axes of the slice: x: 4, y: 4, z: 4, core: 2. Of those that a mesh axis runs over, the one named last changes fastest.
Arguments:
- tokens: bfloat16 [768, 4096], P(None, ('kv', 'tp')), may hold values from -90 to 90
- norm_gain: float32 [4096], P('kv'), may hold values from 0.1 to 1.9
- w_query: bfloat16 [4096, 2048], P('kv', 'tp'), may hold values from -0.09375 to 0.09375
- w_key: bfloat16 [4096, 2048], P('kv', 'tp'), may hold values from -0.09375 to 0.09375
- w_value: bfloat16 [4096, 2048], P('kv', 'tp'), may hold values from -0.09375 to 0.09375
- w_outgate: bfloat16 [4096, 2048], P('kv', 'tp'), may hold values from -0.09375 to 0.09375
- w_igate: bfloat16 [4096, 16], replicated, may hold values from -0.09375 to 0.09375
- w_fgate: bfloat16 [4096, 16], replicated, may hold values from -0.09375 to 0.09375
- forget_bias: float32 [16], P('tp'), may hold values from -1 to 5
- head_gain: float32 [2048], P('tp'), may hold values from 0.1 to 1.9
- w_proj: bfloat16 [2048, 4096], P('tp', 'kv'), may hold values from -0.125 to 0.125
- mixer_gain: float32 [4096], P('kv'), may hold values from 0.1 to 1.9
- w_gate: bfloat16 [4096, 11264], P('kv', 'tp'), may hold values from -0.09375 to 0.09375
- w_up: bfloat16 [4096, 11264], P('kv', 'tp'), may hold values from -0.09375 to 0.09375
- w_down: bfloat16 [11264, 4096], P('tp', 'kv'), may hold values from -0.0546875 to 0.0546875
- state_c: float32 [768, 16, 128, 128], P('kv', 'tp'), may hold values from -0.5 to 0.5
- state_m: float32 [768, 16], P('kv', 'tp'), may hold values from -4 to 4
- tail_keys: bfloat16 [768, 16, 64, 128], P('kv', 'tp'), may hold values from -6 to 6
- tail_values: bfloat16 [768, 16, 64, 128], P('kv', 'tp'), may hold values from -6 to 6
- tail_gate: float32 [768, 16, 64], P('kv', 'tp'), may hold values from -8 to 130
- block_forget: float32 [768, 16], P('kv', 'tp'), may hold values from -6 to 0
- lengths: int32 [768], P('kv'), may hold values from 1 to 64, 12288 in all
Outputs:
- result: bfloat16 [768, 4096], P(None, ('kv', 'tp'))
All inputs are finite; a program needn't handle non-finite values. No bound on the sum of `lengths` on one device may be relied on, other than what follows from the above.
Results may differ from a plain program's by a relative error of at most 0.012.
Values may be sent and summed in bfloat16 or wider, within the bound.
A program may use at most 128 MiB of HBM per device.

v0:
```python
import jax
import jax.numpy as jnp
from jax import lax
from jax.sharding import PartitionSpec as P

D = 4096


EPS = 1e-06


def from_everyone(array, axis):
    copies = jnp.broadcast_to(array, (lax.axis_size(axis), *array.shape))
    return lax.all_to_all(copies, axis, split_axis=0, concat_axis=0, tiled=True)


def joined_along(tiles, dim):
    dims = list(tiles.shape[1:])
    dims[dim] *= tiles.shape[0]
    return jnp.moveaxis(tiles, 0, dim).reshape(dims)


def collect(array, axis, dim):
    tiles = from_everyone(array, axis)
    return joined_along(tiles, dim)


def split_up(array, dim, length):
    dims = array.shape
    tiles = array.reshape(*dims[:dim], length, dims[dim] // length, *dims[dim + 1 :])
    return jnp.moveaxis(tiles, dim, 0)


def summed_on_arrival(array, axis, dim):
    tiles = split_up(array, dim, lax.axis_size(axis))
    arrived = lax.all_to_all(tiles, axis, split_axis=0, concat_axis=0, tiled=True)
    return arrived.sum(axis=0)


def in_one_piece(arrays, axis, dim, along):
    columns = [a.reshape(*a.shape[:along], -1) for a in arrays]
    both = jnp.concatenate(columns, axis=along)
    filled, at, gathered = (summed_on_arrival(both, axis, dim), 0, [])
    for a, column in zip(arrays, columns):
        share = filled[..., at : at + column.shape[along]]
        gathered.append(share.reshape(*share.shape[:along], *a.shape[along:]))
        at += column.shape[along]
    return tuple(gathered)


def taken_together(array, axis):
    everything = from_everyone(array, axis)
    return jnp.sum(everything.astype(jnp.float32), axis=0)


def summed_on_arrival_2(array, axis, dim):
    tiles = split_up(array, dim, lax.axis_size(axis))
    arrived = lax.all_to_all(tiles, axis, split_axis=0, concat_axis=0, tiled=True)
    return arrived.astype(jnp.float32).sum(axis=0)


def recall(
    query,
    key,
    value,
    igate,
    fpre,
    state_c,
    state_m,
    tail_keys,
    tail_values,
    tail_gate,
    block_forget,
    lengths,
):
    f32 = jnp.float32
    span = tail_keys.shape[2]
    head_dim = query.shape[2]
    running = block_forget + jax.nn.log_sigmoid(fpre)
    inter = running + state_m
    live = jnp.arange(span, dtype=jnp.int32)[None, :] < lengths[:, None]
    tail_log = jnp.where(live[:, None, :], running[:, :, None] + tail_gate, -jnp.inf)
    top = jnp.maximum(jnp.maximum(inter, jnp.max(tail_log, axis=2)), igate)
    w_inter = jnp.exp(inter - top)
    w_tail = jnp.exp(tail_log - top[:, :, None])
    w_own = jnp.exp(igate - top)
    scores = jnp.einsum("shpd,shd->shp", tail_keys.astype(f32), query) * head_dim ** (-0.5)
    own = jnp.sum(query * key, axis=2)
    memory = jnp.einsum("shvk,shk->shv", state_c, query)
    weighted = w_tail * scores
    return (
        w_inter[:, :, None] * memory
        + jnp.einsum("shp,shpv->shv", weighted, tail_values.astype(f32))
        + (w_own * own)[:, :, None] * value
    )


def per_device(
    tokens,
    norm_gain,
    w_query,
    w_key,
    w_value,
    w_outgate,
    w_igate,
    w_fgate,
    forget_bias,
    head_gain,
    w_proj,
    mixer_gain,
    w_gate,
    w_up,
    w_down,
    state_c,
    state_m,
    tail_keys,
    tail_values,
    tail_gate,
    block_forget,
    lengths,
):
    f32 = jnp.float32
    bf = jnp.bfloat16
    kv_pos = lax.axis_index("kv")
    tp_pos = lax.axis_index("tp")
    rows = norm_gain.shape[0]
    heads = forget_bias.shape[0]
    head_dim = tail_keys.shape[3]
    seq_dev = lengths.shape[0]
    width = heads * head_dim
    wide = collect(tokens, "tp", 1)
    widef = wide.astype(f32)
    scaled = (widef * norm_gain).astype(bf)

    def local_cols(weight):
        return lax.dynamic_slice(weight, (kv_pos * rows, tp_pos * heads), (rows, heads))

    gate_weights = jnp.concatenate([local_cols(w_igate), local_cols(w_fgate)], axis=1)
    joined = jnp.concatenate([w_query, w_key, w_value, w_outgate], axis=1)
    proj = jnp.dot(scaled, joined, preferred_element_type=f32)
    gates = jnp.dot(scaled, gate_weights, preferred_element_type=f32)
    part_sq = jnp.sum(widef * widef, axis=1)
    proj, gates, sq_rows = in_one_piece((proj, gates, part_sq), "kv", 0, 1)
    inv_first = lax.rsqrt(sq_rows / D + EPS)
    proj = proj * inv_first[:, None]
    gates = gates * inv_first[:, None]
    query = proj[:, :width].reshape(seq_dev, heads, head_dim)
    key = proj[:, width : 2 * width].reshape(seq_dev, heads, head_dim) * head_dim ** (-0.5)
    value = proj[:, 2 * width : 3 * width].reshape(seq_dev, heads, head_dim)
    outgate = proj[:, 3 * width :]
    igate = gates[:, :heads]
    fpre = gates[:, heads:] + forget_bias
    recalled = recall(
        query,
        key,
        value,
        igate,
        fpre,
        state_c,
        state_m,
        tail_keys,
        tail_values,
        tail_gate,
        block_forget,
        lengths,
    )
    normed = recalled * lax.rsqrt(jnp.mean(recalled * recalled, axis=2, keepdims=True) + EPS)
    mixed = (normed.reshape(seq_dev, width) * head_gain * jax.nn.sigmoid(outgate)).astype(bf)
    partial_value = jnp.dot(collect(mixed, "kv", 0), w_proj, preferred_element_type=f32)
    attended = taken_together(partial_value.astype(jnp.bfloat16), "tp").astype(jnp.float32)
    middle = (widef + attended).astype(bf)
    middlef = middle.astype(f32)
    part_sq2 = jnp.sum(middlef * middlef, axis=1)
    scaled_mid = (middlef * mixer_gain).astype(bf)
    gate_part = jnp.dot(scaled_mid, w_gate, preferred_element_type=f32)
    up_part = jnp.dot(scaled_mid, w_up, preferred_element_type=f32)
    gate_sum, up_sum, sq_sum = lax.psum((gate_part, up_part, part_sq2), "kv")
    inv_second = lax.rsqrt(sq_sum / D + EPS)[:, None]
    hidden = (jax.nn.silu(gate_sum * inv_second) * (up_sum * inv_second)).astype(bf)
    down_part = jnp.dot(hidden, w_down, preferred_element_type=f32)
    down_sum = summed_on_arrival_2(down_part.astype(jnp.bfloat16), "tp", 1)
    columns = down_sum.shape[1]
    residual = lax.dynamic_slice_in_dim(middlef, tp_pos * columns, columns, 1)
    return (residual + down_sum).astype(bf)


def solution(mesh):
    return jax.shard_map(
        per_device,
        mesh=mesh,
        in_specs=(
            P(None, ("kv", "tp")),
            P("kv"),
            P("kv", "tp"),
            P("kv", "tp"),
            P("kv", "tp"),
            P("kv", "tp"),
            P(),
            P(),
            P("tp"),
            P("tp"),
            P("tp", "kv"),
            P("kv"),
            P("kv", "tp"),
            P("kv", "tp"),
            P("tp", "kv"),
            P("kv", "tp", None, None),
            P("kv", "tp"),
            P("kv", "tp", None, None),
            P("kv", "tp", None, None),
            P("kv", "tp", None),
            P("kv", "tp"),
            P("kv"),
        ),
        out_specs=P(None, ("kv", "tp")),
        check_vma=False,
    )
```

profile of v0, /device:TPU:1, one launch (start us, length us, event | category | flops | bytes accessed | tf_op | source)
XLA Modules:
  0.0 337.9 jit_solution(16484484869220662567)
XLA Ops:
  6.5 1.7 broadcast_in_dim.18
  8.2 6.1 %all-to-all-start = ((bf16[8,768,32]{1,2,0:T(8,128)(2,1)}), bf16[8,768,32]{1,2,0:T(8,128)(2,1)S(1)}, u32[]{:S(2)}, u32[]{:S(2)}) async-start(bf16[8,768,32]{1,2,0:T(8,128)(2,1)} %broadcast_in_dim.18), calls=%async_computation | async-start | bytes 786432 | tf_op jit(solution)/shard_map/all_to_all | solution.py:14
  14.3 0.8 dynamic_slice.9
  15.1 0.8 dynamic_slice.10
  15.8 6.2 %all-to-all-done = bf16[8,768,32]{1,2,0:T(8,128)(2,1)S(1)} async-done(((bf16[8,768,32]{1,2,0:T(8,128)(2,1)}), bf16[8,768,32]{1,2,0:T(8,128)(2,1)S(1)}, u32[]{:S(2)}, u32[]{:S(2)}) %all-to-all-start) | async-done | bytes 393248 | tf_op jit(solution)/shard_map/all_to_all | solution.py:14
  22.5 2.4 reshape.83
  24.8 2.5 copy.87
  27.6 3.3 fusion.3
  30.9 4.4 %concatenate.15 = f32[16,48,1029]{2,1,0:T(8,128)} concatenate(f32[16,48,1024]{2,1,0:T(8,128)} %fusion.3, f32[16,48,4]{2,1,0:T(8,128)S(1)} %fusion.11, f32[16,48,1]{2,1,0:T(8,128)S(1)} %concatenate.16), dimensions={2} | concatenate | bytes 6322176 | tf_op jit(solution)/shard_map/concatenate | solution.py:42
  35.3 7.8 %all-to-all-start.1 = ((f32[16,48,1029]{2,1,0:T(8,128)}), f32[16,48,1029]{2,1,0:T(8,128)}, u32[]{:S(2)}, u32[]{:S(2)}) async-start(f32[16,48,1029]{2,1,0:T(8,128)} %concatenate.15), calls=%async_computation.1 | async-start | bytes 7077888 | tf_op jit(solution)/shard_map/all_to_all | solution.py:36
  43.2 51.2 %all-to-all-done.1 = f32[16,48,1029]{2,1,0:T(8,128)} async-done(((f32[16,48,1029]{2,1,0:T(8,128)}), f32[16,48,1029]{2,1,0:T(8,128)}, u32[]{:S(2)}, u32[]{:S(2)}) %all-to-all-start.1) | async-done | bytes 3161120 | tf_op jit(solution)/shard_map/all_to_all | solution.py:36
  94.4 2.2 reduce_sum.66
  98.2 2.3 fusion.33
  100.5 4.6 %fusion.32 = f32[48,2,1,128]{3,2,1,0:T(1,128)S(1)} fusion(f32[48,2,128,1]{2,3,1,0:T(1,128)S(1)} %bitcast.57, f32[48,2,128,128]{3,2,1,0:T(8,128)} %param.37), kind=kOutput, calls=%fused_computation.64 | convolution fusion | flops 3145728 | bytes 6389760 | tf_op jit(solution)/shard_map/shvk,shk->shv/dot_general | solution.py:89
  106.2 11.8 %all_to_all.25 = bf16[16,48,256]{2,1,0:T(8,128)(2,1)S(1)} all-to-all(bf16[16,48,256]{2,1,0:T(8,128)(2,1)S(1)} %broadcast_in_dim.21), channel_id=1, replica_groups=mesh['kv'=16,'tp'=8] {'kv'}, dimensions={0} | all-to-all | bytes 786432 | tf_op jit(solution)/shard_map/all_to_all | solution.py:14
  118.6 44.7 %all_to_all.26 = bf16[8,768,256]{2,1,0:T(8,128)(2,1)S(1)} all-to-all(bf16[8,768,256]{2,1,0:T(8,128)(2,1)S(1)} %broadcast_in_dim.22), channel_id=1, replica_groups=mesh['kv'=16,'tp'=8] {'tp'}, dimensions={0} | all-to-all | bytes 6291456 | tf_op jit(solution)/shard_map/all_to_all | solution.py:14
  164.1 4.1 %fusion.28 = f32[768,1408]{1,0:T(8,128)} fusion(bf16[256,1408]{1,0:T(8,128)(2,1)} %param.35, f32[768,256]{0,1:T(8,128)S(1)} %fusion.10, f32[256]{0:T(256)S(1)} %copy-done.4), kind=kOutput, calls=%fused_computation.61 | convolution fusion | flops 554041344 | bytes 5833728 | tf_op jit(solution)/shard_map/dot_general | solution.py:176
  168.2 2.9 fusion.29
  171.2 30.5 %psum.22 = f32[768]{0:T(1024)S(1)} all-reduce(f32[768]{0:T(1024)S(1)} %multiply_reduce_fusion), channel_id=1, replica_groups=mesh['kv'=16,'tp'=8] {'kv'}, use_global_device_ids=true, to_apply=%region_8.9 | all-reduce | flops 768 | bytes 6144 | tf_op jit(solution)/shard_map/psum | solution.py:177
  201.7 109.2 %all-reduce.3.cloned.1.call-done = (f32[768,1408]{1,0:T(8,128)}, f32[768,1408]{1,0:T(8,128)}) async-done(((f32[768,1408]{1,0:T(8,128)}, f32[768,1408]{1,0:T(8,128)}), (f32[768,1408]{1,0:T(8,128)}, f32[768,1408]{1,0:T(8,128)})) %all-reduce.3.cloned.1.call-update) | async-done | bytes 8650768 | tf_op jit(solution)/shard_map/psum | solution.py:177
  310.9 6.0 %fusion.1 = bf16[768,256]{0,1:T(8,128)(2,1)} fusion(bf16[1408,256]{1,0:T(8,128)(2,1)} %param.36, f32[768,1408]{1,0:T(8,128)} %get-tuple-element.5, f32[768,1408]{1,0:T(8,128)} %get-tuple-element.6, f32[768]{0:T(1024)S(1)} %add_rsqrt_fusion.1), kind=kOutput, calls=%fused_computation.4 | convolution fusion | flops 562495488 | bytes 9767936 | tf_op jit(solution)/shard_map/dot_general | solution.py:180
  316.9 5.7 %all-to-all-start.4 = ((bf16[8,768,32]{1,2,0:T(8,128)(2,1)}), bf16[8,768,32]{1,2,0:T(8,128)(2,1)S(1)}, u32[]{:S(2)}, u32[]{:S(2)}) async-start(bf16[8,768,32]{1,2,0:T(8,128)(2,1)} %bitcast.16), calls=%async_computation.4 | async-start | bytes 786432 | tf_op jit(solution)/shard_map/all_to_all | solution.py:58
  322.6 7.7 %all-to-all-done.4 = bf16[8,768,32]{1,2,0:T(8,128)(2,1)S(1)} async-done(((bf16[8,768,32]{1,2,0:T(8,128)(2,1)}), bf16[8,768,32]{1,2,0:T(8,128)(2,1)S(1)}, u32[]{:S(2)}, u32[]{:S(2)}) %all-to-all-start.4) | async-done | bytes 393248 | tf_op jit(solution)/shard_map/all_to_all | solution.py:58
  330.4 0.6 add_convert_fusion.1
  (65 shorter events, 4.8 us)
Async XLA Ops:
  6.5 98.7 %copy-start = (bf16[48,2,64,128]{3,2,1,0:T(8,128)(2,1)S(1)}, bf16[48,2,64,128]{3,2,1,0:T(8,128)(2,1)}, u32[]{:S(2)}) copy-start(bf16[48,2,64,128]{3,2,1,0:T(8,128)(2,1)} %param.40) | copy-start | bytes 4718596
  8.2 19.1 %copy-start.5 = (f32[256]{0:T(256)S(1)}, f32[256]{0:T(256)}, u32[]{:S(2)}) copy-start(f32[256]{0:T(256)} %param.23) | copy-start | bytes 3076
  8.2 13.8 %all-to-all-start = ((bf16[8,768,32]{1,2,0:T(8,128)(2,1)}), bf16[8,768,32]{1,2,0:T(8,128)(2,1)S(1)}, u32[]{:S(2)}, u32[]{:S(2)}) async-start(bf16[8,768,32]{1,2,0:T(8,128)(2,1)} %broadcast_in_dim.18), calls=%async_computation | async-start | bytes 786432 | tf_op jit(solution)/shard_map/all_to_all | solution.py:14
  35.3 7.9 %copy-start.9 = (s32[48]{0:T(128)S(1)}, s32[48]{0:T(128)}, u32[]{:S(2)}) copy-start(s32[48]{0:T(128)} %param.43) | copy-start | bytes 580
  35.3 61.8 %copy-start.7 = (f32[48,2]{0,1:T(2,128)S(1)}, f32[48,2]{0,1:T(2,128)}, u32[]{:S(2)}) copy-start(f32[48,2]{0,1:T(2,128)} %param.38) | copy-start | bytes 1156
  35.3 61.8 %copy-start.8 = (f32[48,2]{0,1:T(2,128)S(1)}, f32[48,2]{0,1:T(2,128)}, u32[]{:S(2)}) copy-start(f32[48,2]{0,1:T(2,128)} %param.42) | copy-start | bytes 1156
  35.3 61.8 %copy-start.10 = (f32[2]{0:T(128)S(1)}, f32[2]{0:T(128)}, u32[]{:S(2)}) copy-start(f32[2]{0:T(128)} %param.30) | copy-start | bytes 28
  35.3 62.0 %copy-start.2 = (f32[48,2,64]{2,1,0:T(2,128)S(1)}, f32[48,2,64]{2,1,0:T(2,128)}, u32[]{:S(2)}) copy-start(f32[48,2,64]{2,1,0:T(2,128)} %param.41) | copy-start | bytes 73732
  35.3 59.1 %all-to-all-start.1 = ((f32[16,48,1029]{2,1,0:T(8,128)}), f32[16,48,1029]{2,1,0:T(8,128)}, u32[]{:S(2)}, u32[]{:S(2)}) async-start(f32[16,48,1029]{2,1,0:T(8,128)} %concatenate.15), calls=%async_computation.1 | async-start | bytes 7077888 | tf_op jit(solution)/shard_map/all_to_all | solution.py:36
  43.1 267.8 %all-reduce.3.cloned.1.call-start = ((), (), s32[]{:S(2)}) async-start(), calls=%async_computation.5 | async-start | bytes 17301504 | tf_op jit(solution)/shard_map/psum | solution.py:177
  100.5 5.7 %copy-start.6 = (f32[256]{0:T(256)S(1)}, f32[256]{0:T(256)}, u32[]{:S(2)}) copy-start(f32[256]{0:T(256)} %param.31) | copy-start | bytes 3076
  100.5 17.6 %copy-start.3 = (bf16[256,256]{1,0:T(8,128)(2,1)S(1)}, bf16[256,256]{1,0:T(8,128)(2,1)}, u32[]{:S(2)}) copy-start(bf16[256,256]{1,0:T(8,128)(2,1)} %param.32) | copy-start | bytes 393220
  163.3 0.8 copy-start.4
  164.0 4.2 %copy-start.1 = (bf16[256,1408]{1,0:T(8,128)(2,1)S(1)}, bf16[256,1408]{1,0:T(8,128)(2,1)}, u32[]{:S(2)}) copy-start(bf16[256,1408]{1,0:T(8,128)(2,1)} %param.34) | copy-start | bytes 2162692
  316.9 13.4 %all-to-all-start.4 = ((bf16[8,768,32]{1,2,0:T(8,128)(2,1)}), bf16[8,768,32]{1,2,0:T(8,128)(2,1)S(1)}, u32[]{:S(2)}, u32[]{:S(2)}) async-start(bf16[8,768,32]{1,2,0:T(8,128)(2,1)} %bitcast.16), calls=%async_computation.4 | async-start | bytes 786432 | tf_op jit(solution)/shard_map/all_to_all | solution.py:58
Sparse Core Ops, SparseCore 0:
  171.2 139.6 all-reduce.2
where the time goes:
time: 339 us; the launch traced here: 338 us
  waiting for transfers between devices  174 us (51%)
  blocking collectives  87 us (26%)
  matrix products  24.2 us (7%)
  starting transfers between devices  19.6 us (6%)
  local copies, waits for them, and re-layouts  14 us (4%)
  between operations  13.7 us (4%)
  other arithmetic  5.07 us (1%)
    psum x1, waiting for transfers between devices, per_device(): gate_sum, up_sum, sq_sum = lax.psum((gate_part, up_part, part_sq2), 'kv')  109 us
    all_to_all x2, blocking collectives, from_everyone(): return lax.all_to_all(copies, axis, split_axis=0, concat_axis=0, tiled=True)  56.5 us
    all_to_all x1, waiting for transfers between devices, summed_on_arrival(): lax.all_to_all(tiles, axis, split_axis=0, concat_axis=0, tiled=True)  51.2 us
    psum x1, blocking collectives, per_device(): gate_sum, up_sum, sq_sum = lax.psum((gate_part, up_part, part_sq2), 'kv')  30.5 us
    all_to_all x1, starting transfers between devices, summed_on_arrival(): lax.all_to_all(tiles, axis, split_axis=0, concat_axis=0, tiled=True)  7.79 us
    all_to_all x1, waiting for transfers between devices, summed_on_arrival_2(): lax.all_to_all(tiles, axis, split_axis=0, concat_axis=0, tiled=True)  7.7 us
  transfers between devices with their start and end apart: 4, of which 4 were waited for; matrix products, arithmetic and copies ran while one was open for 1% of the time, Pallas kernels for 0%

commit v1 on v0

v1 whole, which is shorter than its diff:
```python
import jax
import jax.numpy as jnp
from jax import lax
from jax.experimental import pallas as pl
from jax.experimental.pallas import tpu as pltpu
from jax.sharding import PartitionSpec as P

D = 4096
EPS = 1e-06
F32 = jnp.float32
BF = jnp.bfloat16
MESH = pl.DeviceIdType.MESH
N1 = 1024
N2 = 2816
FFD = 1408


def remote(src, dst, ss, rs, dev):
    return pltpu.make_async_remote_copy(
        src_ref=src, dst_ref=dst, send_sem=ss, recv_sem=rs, device_id=dev, device_id_type=MESH
    )


def mod4(v):
    return lax.rem(v, 4)


def transpose_padded(rows):
    missing = 128 - rows.shape[0]
    if missing:
        rows = jnp.concatenate([rows, jnp.zeros((missing, rows.shape[1]), F32)], axis=0)
    return rows.T


def column_of(row):
    return jnp.broadcast_to(row, (128, 128)).T


def layer(
    tokens, norm_gain, w_query, w_key, w_value, w_outgate, w_igate, w_fgate, head_gain, w_proj,
    mixer_gain, w_gate, w_up, w_down, state_c, tail_keys, tail_values, tail_gate, meta,
    out,
    tok_v, wide_t, wide, scaled, wqkvo, wig_v, wfg_v, wproj_v, wgu, wdown_v, cbuf, kbuf, vbuf,
    gsend, grecv,
    a_p, a_own, a_in, a_comb, a_l, a_r, a_q, a_qin, a_qcomb, a_ql, a_qr,
    qs, tailo, mix_all, att_send, att_recv, mid_all, scaled_mid, ssend, srecv, mid_sel,
    b_p, b_own, b_in, b_comb, b_l, b_r, b_q, b_qin, b_qcomb, b_ql, b_qr,
    hid, fsend, frecv,
    lsem, tok_s, tok_r, g_s, g_r, mix_s, mix_r, att_s, att_r, mid_s, mid_r, sq_s, sq_r,
    ra_s, ra_r, rb_s, rb_r, h_s, h_r, f_s, f_r,
):
    kv = lax.axis_index("kv")
    tp = lax.axis_index("tp")
    z = lax.div(kv, 4)
    x = lax.rem(kv, 4)
    c = lax.rem(tp, 2)
    pa = x * (1 - c) + z * c
    pb = z * (1 - c) + x * c

    def kv_of(ia, ib):
        return ia * (1 + 3 * c) + ib * (4 - 3 * c)

    def at_a(g):
        return (kv_of(mod4(pa + g), pb), tp)

    def at_b(g):
        return (kv_of(pa, mod4(pb + g)), tp)

    def kv_peer(i):
        return mod4(z + i // 4) * 4 + mod4(x + i % 4)

    def kv_from(i):
        return mod4(z + 4 - i // 4) * 4 + mod4(x + 4 - i % 4)

    def tp_peer(r):
        return lax.rem(tp + r, 8)

    def tp_from(r):
        return lax.rem(tp + 8 - r, 8)

    def rows48(k):
        return pl.ds(pl.multiple_of(k * 48, 16), 48)

    def rows96(k):
        return pl.ds(pl.multiple_of(k * 96, 32), 96)

    def rows32(k):
        return pl.ds(pl.multiple_of(k * 32, 32), 32)

    sends = []

    def send(*args):
        copy = remote(*args)
        copy.start()
        sends.append(copy)

    loads = [
        pltpu.make_async_copy(tokens, tok_v, lsem.at[0]),
        pltpu.make_async_copy(w_query, wqkvo.at[:, pl.ds(0, 256)], lsem.at[1]),
        pltpu.make_async_copy(w_key, wqkvo.at[:, pl.ds(256, 256)], lsem.at[2]),
        pltpu.make_async_copy(w_value, wqkvo.at[:, pl.ds(512, 256)], lsem.at[3]),
        pltpu.make_async_copy(w_outgate, wqkvo.at[:, pl.ds(768, 256)], lsem.at[4]),
        pltpu.make_async_copy(w_igate.at[pl.ds(pl.multiple_of(kv * 256, 256), 256)], wig_v, lsem.at[5]),
        pltpu.make_async_copy(w_fgate.at[pl.ds(pl.multiple_of(kv * 256, 256), 256)], wfg_v, lsem.at[6]),
        pltpu.make_async_copy(state_c, cbuf, lsem.at[7]),
        pltpu.make_async_copy(tail_keys, kbuf, lsem.at[8]),
        pltpu.make_async_copy(tail_values, vbuf, lsem.at[9]),
        pltpu.make_async_copy(w_proj, wproj_v, lsem.at[10]),
        pltpu.make_async_copy(w_gate, wgu.at[:, pl.ds(0, FFD)], lsem.at[11]),
        pltpu.make_async_copy(w_up, wgu.at[:, pl.ds(FFD, FFD)], lsem.at[12]),
        pltpu.make_async_copy(w_down, wdown_v, lsem.at[13]),
    ]
    for load in loads:
        load.start()

    barrier = pltpu.get_barrier_semaphore()
    for i in range(1, 16):
        pl.semaphore_signal(barrier, inc=1, device_id=(kv_peer(i), tp), device_id_type=MESH)
    for r in range(1, 8):
        pl.semaphore_signal(barrier, inc=1, device_id=(kv, tp_peer(r)), device_id_type=MESH)

    loads[0].wait()
    tok_f = tok_v[...].astype(F32)
    wide_t[rows32(tp), :] = tok_f.T.astype(BF)
    pl.semaphore_wait(barrier, 22)

    for r in range(1, 8):
        mine = wide_t.at[rows32(tp)]
        send(mine, mine, tok_s.at[r], tok_r.at[r], (kv, tp_peer(r)))

    lane = lax.broadcasted_iota(jnp.int32, (128, 128), 1)
    for i in range(5, 7):
        loads[i].wait()
    grow = lax.broadcasted_iota(jnp.int32, (16, 128), 0)
    glane = lax.broadcasted_iota(jnp.int32, (16, 128), 1)
    pick_i = jnp.where((glane < 2) & (grow == 2 * tp + glane), 1.0, 0.0).astype(BF)
    pick_f = jnp.where((glane >= 2) & (glane < 4) & (grow == 2 * tp + glane - 2), 1.0, 0.0).astype(BF)
    gate_w = (
        jnp.dot(wig_v[...], pick_i, preferred_element_type=F32)
        + jnp.dot(wfg_v[...], pick_f, preferred_element_type=F32)
    ).astype(BF)
    forget_row = meta[0:1, :]
    state_row = meta[1:2, :]
    length_row = meta[2:3, :]
    bias_row = meta[3:4, :]
    tg = transpose_padded(tail_gate[...])
    lane64 = lax.broadcasted_iota(jnp.int32, (64, 128), 1)
    gate_t = jnp.where(lane64 < 64, tg[:64], pltpu.roll(tg[64:], 64, 1))

    for r in range(1, 8):
        src = wide_t.at[rows32(tp_from(r))]
        remote(src, src, tok_s.at[r], tok_r.at[r], (kv, tp)).wait_recv()
    for b in range(6):
        block = wide_t[:, 128 * b : 128 * b + 128].astype(F32).T
        wide[128 * b : 128 * b + 128, :] = block.astype(BF)
        scaled[128 * b : 128 * b + 128, :] = (block * norm_gain[...]).astype(BF)

    def ring_sum(lhs, weights, n, tile, p, own, inn, comb, from_l, from_r, q, qin, qcomb, ql, qr, ss, rs, between):
        half = n // 2
        first, second = pl.ds(0, half), pl.ds(half, half)

        def group(g, put):
            ia = mod4(pa + g)
            rows = jnp.concatenate([lhs[rows48(kv_of(ia, ib)), :] for ib in range(4)], axis=0)

            def step(t, _):
                cols = pl.ds(pl.multiple_of(t * tile, tile), tile)
                put(cols, jnp.dot(rows, weights[:, cols], preferred_element_type=F32))
                return 0

            lax.fori_loop(0, n // tile, step, 0)

        def into(ref):
            def put(cols, value):
                ref[:, cols] = value.astype(ref.dtype)

            return put

        def add_rows(count, fn):
            def step(i, _):
                fn(pl.ds(pl.multiple_of(i * 16, 16), 16))
                return 0

            lax.fori_loop(0, count // 16, step, 0)

        def waited(dst, i):
            remote(dst, dst, ss.at[i], rs.at[i], (kv, tp)).wait_recv()

        right, left = at_a(1), at_a(3)
        group(2, into(p.at[0]))
        send(p.at[0, :, first], inn.at[0], ss.at[0], rs.at[0], right)
        send(p.at[0, :, second], inn.at[1], ss.at[1], rs.at[1], left)
        group(1, into(p.at[1]))
        send(p.at[1, :, second], from_l.at[:, second], ss.at[2], rs.at[2], right)
        group(3, into(p.at[2]))
        send(p.at[2, :, first], from_r.at[:, first], ss.at[3], rs.at[3], left)
        group(0, into(own))
        between()
        waited(inn.at[0], 0)

        def comb0(rows):
            comb[0, rows, :] = (p[1, rows, first].astype(F32) + inn[0, rows, :].astype(F32)).astype(BF)

        add_rows(192, comb0)
        send(comb.at[0], from_l.at[:, first], ss.at[4], rs.at[4], right)
        waited(inn.at[1], 1)

        def comb1(rows):
            comb[1, rows, :] = (p[2, rows, second].astype(F32) + inn[1, rows, :].astype(F32)).astype(BF)

        add_rows(192, comb1)
        send(comb.at[1], from_r.at[:, second], ss.at[5], rs.at[5], left)
        waited(from_l.at[:, second], 2)
        waited(from_r.at[:, first], 3)
        waited(from_l.at[:, first], 4)
        waited(from_r.at[:, second], 5)

        right, left = at_b(1), at_b(3)

        def total(g, put):
            base = mod4(pb + g) * 48
            for i in range(3):
                rows = pl.ds(pl.multiple_of(base + 16 * i, 16), 16)
                put(
                    pl.ds(16 * i, 16),
                    own[rows, :] + from_l[rows, :].astype(F32) + from_r[rows, :].astype(F32),
                )

        def into_q(j):
            def put(rows, value):
                q[j, rows, :] = value.astype(BF)

            return put

        total(2, into_q(0))
        send(q.at[0, :, first], qin.at[0], ss.at[6], rs.at[6], right)
        send(q.at[0, :, second], qin.at[1], ss.at[7], rs.at[7], left)
        total(1, into_q(1))
        send(q.at[1, :, second], ql.at[:, second], ss.at[8], rs.at[8], right)
        total(3, into_q(2))
        send(q.at[2, :, first], qr.at[:, first], ss.at[9], rs.at[9], left)
        waited(qin.at[0], 6)
        qcomb[0] = (q[1, :, first].astype(F32) + qin[0].astype(F32)).astype(BF)
        send(qcomb.at[0], ql.at[:, first], ss.at[10], rs.at[10], right)
        waited(qin.at[1], 7)
        qcomb[1] = (q[2, :, second].astype(F32) + qin[1].astype(F32)).astype(BF)
        send(qcomb.at[1], qr.at[:, second], ss.at[11], rs.at[11], left)
        mine = pl.ds(pl.multiple_of(pb * 48, 16), 48)
        waited(ql.at[:, second], 8)
        waited(qr.at[:, first], 9)
        waited(ql.at[:, first], 10)
        waited(qr.at[:, second], 11)

        def result(cols):
            return (
                own[mine, cols]
                + from_l[mine, cols].astype(F32)
                + from_r[mine, cols].astype(F32)
                + ql[:, cols].astype(F32)
                + qr[:, cols].astype(F32)
            )

        return result

    def small_sum(recv_ref, own_tile, ss, rs):
        acc = own_tile
        for i in range(1, 16):
            remote(recv_ref.at[i], recv_ref.at[i], ss.at[i], rs.at[i], (kv, tp)).wait_recv()
            acc = acc + recv_ref[i]
        return acc

    lane48 = lax.broadcasted_iota(jnp.int32, (48, 128), 1)

    def gate_tiles():
        def step(k, _):
            rows = rows48(k)
            part = jnp.dot(scaled[rows, :], gate_w, preferred_element_type=F32)
            wf = wide[rows, :].astype(F32)
            sq = jnp.sum(wf * wf, axis=1, keepdims=True)
            gsend[k] = transpose_padded(jnp.where(lane48 == 4, sq, part))[:8]
            return 0

        lax.fori_loop(0, 16, step, 0)
        for i in range(1, 16):
            k = kv_peer(i)
            send(gsend.at[k], grecv.at[i], g_s.at[i], g_r.at[i], (k, tp))

    for i in range(1, 5):
        loads[i].wait()
    proj = ring_sum(
        scaled, wqkvo, N1, 256, a_p, a_own, a_in, a_comb, a_l, a_r, a_q, a_qin, a_qcomb, a_ql, a_qr,
        ra_s, ra_r, gate_tiles,
    )
    gsum = small_sum(grecv, gsend[kv], g_s, g_r)
    inv_row = lax.rsqrt(gsum[4:5, :] / D + EPS)
    inv_col = column_of(inv_row)[:48]
    lane8 = lax.broadcasted_iota(jnp.int32, (8, 128), 1)

    def pair_row(first, second):
        a8 = jnp.broadcast_to(first, (8, 128))
        b8 = jnp.broadcast_to(second, (8, 128))
        return jnp.where(lane8 < 64, a8, pltpu.roll(b8, 64, 1))

    igate = pair_row(gsum[0:1, :] * inv_row, gsum[1:2, :] * inv_row)
    fpre = pair_row(gsum[2:3, :] * inv_row, gsum[3:4, :] * inv_row) + bias_row
    log_sig = -(jnp.maximum(-fpre, 0.0) + jnp.log1p(jnp.exp(-jnp.abs(fpre))))
    running = forget_row + log_sig
    inter = running + state_row
    pos = lax.broadcasted_iota(jnp.int32, (64, 128), 0).astype(F32)
    tail_log = jnp.where(pos < length_row, running[0:1] + gate_t, -jnp.inf)
    top = jnp.maximum(jnp.maximum(inter[0:1], jnp.max(tail_log, axis=0, keepdims=True)), igate[0:1])
    w_inter = jnp.exp(inter[0:1] - top)
    w_own = column_of(jnp.exp(igate[0:1] - top))
    w_tail = jnp.exp(tail_log - top)

    for h in range(2):
        qs[h] = proj(pl.ds(128 * h, 128)) * inv_col
    for i in range(7, 10):
        loads[i].wait()

    def recall_step(s, carry):
        mem_t, sc_t = carry
        for h in range(2):
            qrow = qs[h, pl.ds(s, 1), :]
            m = jnp.sum(cbuf[s, h] * qrow, axis=1, keepdims=True)
            mem_t = jnp.where(lane == 64 * h + s, m, mem_t)
            sc = jnp.sum(kbuf[s, h].astype(F32) * qrow, axis=1, keepdims=True)
            sc_t = jnp.where(lane64 == 64 * h + s, sc, sc_t)
        return mem_t, sc_t

    mem_t, sc_t = lax.fori_loop(
        0, 48, recall_step, (jnp.zeros((128, 128), F32), jnp.zeros((64, 128), F32))
    )
    weighted = w_tail * (sc_t * 128 ** (-0.5))

    def tail_step(s, _):
        for h in range(2):
            wcol = jnp.sum(jnp.where(lane64 == 64 * h + s, weighted, 0.0), axis=1, keepdims=True)
            tailo[h, pl.ds(s, 1), :] = jnp.sum(vbuf[s, h].astype(F32) * wcol, axis=0, keepdims=True)
        return 0

    lax.fori_loop(0, 48, tail_step, 0)
    memory = (mem_t * w_inter).T
    mixed = []
    for h in range(2):
        q = qs[h]
        k = proj(pl.ds(256 + 128 * h, 128)) * inv_col * 128 ** (-0.5)
        v = proj(pl.ds(512 + 128 * h, 128)) * inv_col
        og = proj(pl.ds(768 + 128 * h, 128)) * inv_col
        own = jnp.sum(q * k, axis=1, keepdims=True)
        recalled = memory[64 * h : 64 * h + 48] + tailo[h] + w_own[64 * h : 64 * h + 48] * own * v
        ms = jnp.mean(recalled * recalled, axis=1, keepdims=True)
        normed = recalled * lax.rsqrt(ms + EPS)
        hg = head_gain[:, 128 * h : 128 * h + 128]
        mixed.append((normed * hg * (1.0 / (1.0 + jnp.exp(-og)))).astype(BF))
    mix_all[rows48(kv), :] = jnp.concatenate(mixed, axis=1)
    for i in range(1, 16):
        mine = mix_all.at[rows48(kv)]
        send(mine, mine, mix_s.at[i], mix_r.at[i], (kv_peer(i), tp))
    loads[10].wait()
    for i in range(1, 16):
        src = mix_all.at[rows48(kv_from(i))]
        remote(src, src, mix_s.at[i], mix_r.at[i], (kv, tp)).wait_recv()

    for r in [4, 3, 5, 2, 6, 1, 7, 0]:
        part = jnp.dot(mix_all[rows96(tp_peer(r)), :], wproj_v[...], preferred_element_type=F32)
        att_send[r] = part.astype(BF)
        if r:
            send(att_send.at[r], att_recv.at[r], att_s.at[r], att_r.at[r], (kv, tp_peer(r)))
    attended = att_send[0].astype(F32)
    for r in range(1, 8):
        remote(att_recv.at[r], att_recv.at[r], att_s.at[r], att_r.at[r], (kv, tp)).wait_recv()
        attended = attended + att_recv[r].astype(F32)
    mid_all[rows96(tp), :] = (wide[rows96(tp), :].astype(F32) + attended).astype(BF)
    for r in [4, 3, 5, 2, 6, 1, 7]:
        mine = mid_all.at[rows96(tp)]
        send(mine, mine, mid_s.at[r], mid_r.at[r], (kv, tp_peer(r)))
    for r in range(1, 8):
        src = mid_all.at[rows96(tp_from(r))]
        remote(src, src, mid_s.at[r], mid_r.at[r], (kv, tp)).wait_recv()

    def scale_mid(k, _):
        rows = rows48(k)
        m = mid_all[rows, :].astype(F32)
        scaled_mid[rows, :] = (m * mixer_gain[...]).astype(BF)
        return 0

    lax.fori_loop(0, 16, scale_mid, 0)

    def square_tiles():
        def step(k, _):
            m = mid_all[rows48(k), :].astype(F32)
            sq = m * m
            row = jnp.sum(transpose_padded(sq[:, :128] + sq[:, 128:]), axis=0, keepdims=True)
            ssend[k] = jnp.broadcast_to(row, (8, 128))
            return 0

        lax.fori_loop(0, 16, step, 0)
        for i in range(1, 16):
            k = kv_peer(i)
            send(ssend.at[k], srecv.at[i], sq_s.at[i], sq_r.at[i], (k, tp))
        srow = lax.broadcasted_iota(jnp.int32, (256, 128), 0)
        slane = lax.broadcasted_iota(jnp.int32, (256, 128), 1)
        pick = jnp.where((slane < 32) & (srow == 32 * tp + slane), 1.0, 0.0).astype(BF)
        mid_sel[...] = jnp.dot(mid_all[...], pick, preferred_element_type=F32)

    loads[11].wait()
    loads[12].wait()
    both = ring_sum(
        scaled_mid, wgu, N2, 256, b_p, b_own, b_in, b_comb, b_l, b_r, b_q, b_qin, b_qcomb, b_ql, b_qr,
        rb_s, rb_r, square_tiles,
    )
    ssum = small_sum(srecv, ssend[kv], sq_s, sq_r)
    inv_mid = column_of(lax.rsqrt(ssum[0:1] / D + EPS))[:48]

    def hidden_step(t, _):
        cols = pl.ds(pl.multiple_of(t * 128, 128), 128)
        gate = both(cols) * inv_mid
        up = both(pl.ds(pl.multiple_of(t * 128 + FFD, 128), 128)) * inv_mid
        hid[rows48(kv), cols] = (gate * (1.0 / (1.0 + jnp.exp(-gate))) * up).astype(BF)
        return 0

    lax.fori_loop(0, FFD // 128, hidden_step, 0)

    part_rows = (pl.ds(0, 32), pl.ds(32, 16))

    def chunk(ra, rb):
        return hid.at[rows48(kv_of(mod4(pa + 4 - ra), mod4(pb + 4 - rb)))]

    def piece(ref, i):
        return ref.at[part_rows[i]]

    def hop(ref, i, dev):
        send(ref, ref, h_s.at[i], h_r.at[i], dev)

    def arrived(ref, i):
        remote(ref, ref, h_s.at[i], h_r.at[i], (kv, tp)).wait_recv()

    def spread(rb):
        hop(chunk(0, rb), 4 + rb, at_a(1))
        hop(chunk(0, rb), 8 + rb, at_a(3))

    hop(chunk(0, 0), 0, at_b(1))
    hop(chunk(0, 0), 1, at_b(3))
    spread(0)
    arrived(chunk(0, 1), 0)
    hop(piece(chunk(0, 1), 0), 2, at_b(1))
    spread(1)
    arrived(chunk(0, 3), 1)
    hop(piece(chunk(0, 3), 1), 3, at_b(3))
    spread(3)
    arrived(chunk(1, 0), 4)
    hop(chunk(1, 0), 12, at_a(1))
    arrived(piece(chunk(0, 2), 0), 2)
    arrived(piece(chunk(0, 2), 1), 3)
    spread(2)
    arrived(chunk(1, 1), 5)
    hop(chunk(1, 1), 13, at_a(1))
    arrived(chunk(3, 3), 11)
    hop(chunk(3, 3), 15, at_a(3))
    arrived(chunk(3, 2), 10)
    hop(chunk(3, 2), 14, at_a(3))
    loads[13].wait()
    arrived(chunk(1, 2), 6)
    arrived(chunk(1, 3), 7)
    arrived(chunk(3, 0), 8)
    arrived(chunk(3, 1), 9)
    for rb in range(4):
        arrived(chunk(2, rb), 12 + rb)

    for b in range(6):
        part = jnp.dot(hid[128 * b : 128 * b + 128, :], wdown_v[...], preferred_element_type=F32)
        fsend[:, 128 * b : 128 * b + 128] = part.T.astype(BF)
    for r in [4, 3, 5, 2, 6, 1, 7]:
        t = tp_peer(r)
        send(fsend.at[rows32(t)], frecv.at[r], f_s.at[r], f_r.at[r], (kv, t))
    total = fsend[rows32(tp), :].astype(F32)
    for r in range(1, 8):
        remote(frecv.at[r], frecv.at[r], f_s.at[r], f_r.at[r], (kv, tp)).wait_recv()
        total = total + frecv[r].astype(F32)
    for b in range(6):
        down = transpose_padded(total[:, 128 * b : 128 * b + 128])
        rows = slice(128 * b, 128 * b + 128)
        out[rows, :] = (mid_sel[rows, :] + down)[:, :32].astype(BF)
    for copy in sends:
        copy.wait_send()


def per_device(
    tokens, norm_gain, w_query, w_key, w_value, w_outgate, w_igate, w_fgate, forget_bias, head_gain,
    w_proj, mixer_gain, w_gate, w_up, w_down, state_c, state_m, tail_keys, tail_values, tail_gate,
    block_forget, lengths,
):
    def pair_row(a):
        return jnp.pad(a.T, ((0, 0), (0, 16))).reshape(1, 128)

    length_row = pair_row(jnp.broadcast_to(lengths.astype(F32)[:, None], (48, 2)))
    bias_row = pair_row(jnp.broadcast_to(forget_bias[None, :], (48, 2)))
    meta = jnp.concatenate(
        [pair_row(block_forget), pair_row(state_m), length_row, bias_row, jnp.zeros((4, 128), F32)], axis=0
    )
    any_spec = pl.BlockSpec(memory_space=pl.ANY)
    vm_spec = pl.BlockSpec(memory_space=pltpu.VMEM)
    dma = pltpu.SemaphoreType.DMA

    def ring_bufs(n):
        return [
            pltpu.VMEM((3, 192, n), BF),
            pltpu.VMEM((192, n), F32),
            pltpu.VMEM((2, 192, n // 2), BF),
            pltpu.VMEM((2, 192, n // 2), BF),
            pltpu.VMEM((192, n), BF),
            pltpu.VMEM((192, n), BF),
            pltpu.VMEM((3, 48, n), BF),
            pltpu.VMEM((2, 48, n // 2), BF),
            pltpu.VMEM((2, 48, n // 2), BF),
            pltpu.VMEM((48, n), BF),
            pltpu.VMEM((48, n), BF),
        ]

    scratch = [
        pltpu.VMEM((768, 32), BF),
        pltpu.VMEM((256, 768), BF),
        pltpu.VMEM((768, 256), BF),
        pltpu.VMEM((768, 256), BF),
        pltpu.VMEM((256, N1), BF),
        pltpu.VMEM((256, 16), BF),
        pltpu.VMEM((256, 16), BF),
        pltpu.VMEM((256, 256), BF),
        pltpu.VMEM((256, N2), BF),
        pltpu.VMEM((FFD, 256), BF),
        pltpu.VMEM((48, 2, 128, 128), F32),
        pltpu.VMEM((48, 2, 64, 128), BF),
        pltpu.VMEM((48, 2, 64, 128), BF),
        pltpu.VMEM((16, 8, 128), F32),
        pltpu.VMEM((16, 8, 128), F32),
        *ring_bufs(N1),
        pltpu.VMEM((2, 48, 128), F32),
        pltpu.VMEM((2, 48, 128), F32),
        pltpu.VMEM((768, 256), BF),
        pltpu.VMEM((8, 96, 256), BF),
        pltpu.VMEM((8, 96, 256), BF),
        pltpu.VMEM((768, 256), BF),
        pltpu.VMEM((768, 256), BF),
        pltpu.VMEM((16, 8, 128), F32),
        pltpu.VMEM((16, 8, 128), F32),
        pltpu.VMEM((768, 128), F32),
        *ring_bufs(N2),
        pltpu.VMEM((768, FFD), BF),
        pltpu.VMEM((256, 768), BF),
        pltpu.VMEM((8, 32, 768), BF),
        dma((14,)),
        dma((8,)), dma((8,)),
        dma((16,)), dma((16,)),
        dma((16,)), dma((16,)),
        dma((8,)), dma((8,)),
        dma((8,)), dma((8,)),
        dma((16,)), dma((16,)),
        dma((12,)), dma((12,)),
        dma((12,)), dma((12,)),
        dma((16,)), dma((16,)),
        dma((8,)), dma((8,)),
    ]
    specs = [any_spec] * 19
    for i in (1, 8, 10, 17, 18):
        specs[i] = vm_spec
    return pl.pallas_call(
        layer,
        out_shape=jax.ShapeDtypeStruct((768, 32), BF),
        in_specs=specs,
        out_specs=vm_spec,
        scratch_shapes=scratch,
        compiler_params=pltpu.CompilerParams(
            collective_id=0, has_side_effects=True, vmem_limit_bytes=60 * 1024 * 1024
        ),
    )(
        tokens, norm_gain.reshape(1, 256), w_query, w_key, w_value, w_outgate, w_igate, w_fgate,
        head_gain.reshape(1, 256), w_proj, mixer_gain.reshape(1, 256), w_gate, w_up, w_down,
        state_c, tail_keys, tail_values, tail_gate.reshape(48, 128), meta,
    )


def solution(mesh):
    kvtp = P("kv", "tp")
    return jax.shard_map(
        per_device,
        mesh=mesh,
        in_specs=(
            P(None, ("kv", "tp")), P("kv"), kvtp, kvtp, kvtp, kvtp, P(), P(), P("tp"), P("tp"),
            P("tp", "kv"), P("kv"), kvtp, kvtp, P("tp", "kv"), P("kv", "tp", None, None), kvtp,
            P("kv", "tp", None, None), P("kv", "tp", None, None), P("kv", "tp", None), kvtp, P("kv"),
        ),
        out_specs=P(None, ("kv", "tp")),
        check_vma=False,
    )
```

time: 339 us -> 135 us (0.40)
  waiting for transfers between devices: 174 us -> 0 us
  Pallas kernels: 0 us -> 123 us
  blocking collectives: 87 us -> 0 us
  matrix products: 24.2 us -> 0 us
  starting transfers between devices: 19.6 us -> 0 us
  between operations: 13.7 us -> 0.02 us
  other arithmetic: 5.07 us -> 0.69 us
    pallas_call x0 -> x1, Pallas kernels: none -> 123 us  [per_device(): pl.pallas_call(layer, out_shape=jax.ShapeDtypeStruct((768, 32), BF), in_s...]
    psum x1 -> x0, waiting for transfers between devices: 109 us -> none  [per_device(): gate_sum, up_sum, sq_sum = lax.psum((gate_part, up_part, part_sq2), 'kv')]
    all_to_all x3 -> x0, waiting for transfers between devices: 65.1 us -> none  [the longest x1 51.2 us: summed_on_arrival(): lax.all_to_all(tiles, axis, split_axis=0, concat_axis=0, tiled=True)]
    all_to_all x2 -> x0, blocking collectives: 56.5 us -> none  [from_everyone(): return lax.all_to_all(copies, axis, split_axis=0, concat_axis=0, tiled=True)]
    psum x1 -> x0, blocking collectives: 30.5 us -> none  [per_device(): gate_sum, up_sum, sq_sum = lax.psum((gate_part, up_part, part_sq2), 'kv')]
    dot_general x9 -> x0, matrix products: 24.2 us -> none  [the longest x1 6.03 us: per_device(): down_part = jnp.dot(hidden, w_down, preferred_element_type=f32)]
    all_to_all x3 -> x0, starting transfers between devices: 19.6 us -> none  [the longest x1 7.79 us: summed_on_arrival(): lax.all_to_all(tiles, axis, split_axis=0, concat_axis=0, tiled=True)]
    unnamed x23 -> x5, local copies, waits for them, and re-layouts: 0.12 us -> 5.25 us
  transfers between devices with their start and end apart: 4 -> 0, of which waited for: 4 -> 0; matrix products, arithmetic and copies ran while one was open for 1% -> 0% of each run, Pallas kernels for 0% -> 0%
where the time goes in v1:
time: 135 us
  Pallas kernels  123 us (91%)
  local copies, waits for them, and re-layouts  11.5 us (9%)
    pallas_call x1, Pallas kernels, per_device(): pl.pallas_call(layer, out_shape=jax.ShapeDtypeStruct((768, 32), BF), in_s...  123 us
    unnamed x5, local copies, waits for them, and re-layouts  5.25 us

profile of v1, /device:TPU:1, one launch (start us, length us, event | category | flops | bytes accessed | tf_op | source)
XLA Modules:
  0.0 134.7 jit_solution(3922663390169054579)
XLA Ops:
  0.0 0.0 copy-start
  0.0 0.7 convert_element_type.8
  0.7 0.1 reshape.32
  0.8 0.7 transpose.15
  1.5 0.1 reshape.33
  1.6 0.7 pad.16
  2.3 0.1 reshape.31
  2.4 0.7 pad.15
  3.1 0.1 reshape.30
  3.1 0.6 concatenate.3.meta
  3.8 1.5 %reshape.29.tail_gate = f32[48,128]{1,0:T(8,128)} reshape(f32[48,2,64]{2,1,0:T(2,128)} %param.41) | data formatting | bytes 49152 | tf_op jit(solution)/shard_map/reshape | solution.py:579
  5.3 1.6 %copy.23.tokens = bf16[768,32]{1,0:T(8,128)(2,1)} copy(bf16[768,32]{0,1:T(8,128)(2,1)} %param.22) | data formatting | bytes 98304 | tf_op args[0]
  6.9 2.2 %copy.24.w_igate = bf16[4096,16]{1,0:T(8,128)(2,1)} copy(bf16[4096,16]{0,1:T(8,128)(2,1)} %param.28) | data formatting | bytes 262144 | tf_op args[6]
  9.1 0.0 copy-done
  9.1 1.4 %copy.25.w_fgate = bf16[4096,16]{1,0:T(8,128)(2,1)} copy(bf16[4096,16]{0,1:T(8,128)(2,1)S(1)} %copy-done) | data formatting | bytes 262144 | tf_op args[7]
  10.5 122.5 %shard_map.208 = bf16[768,32]{1,0:T(8,128)(2,1)} custom-call(bf16[768,32]{1,0:T(8,128)(2,1)} %copy.23.tokens, f32[1,256]{1,0:T(1,128)} %bitcast.5, bf16[256,256]{1,0:T(8,128)(2,1)} %w_query.1, bf16[256,256]{1,0:T(8,128)(2,1)} %w_key.1, bf16[256,256]{1,0:T(8,128)(2,1)} %w_value.1, bf16[256,256]{1,0:T(8,128)(2,1)} %w_outgate.1, ...), custom_call_target="tpu_custom_call" | custom-call | tf_op jit(solution)/shard_map/pallas_call | solution.py:567
  133.1 1.7 %copy.26 = bf16[768,32]{0,1:T(8,128)(2,1)} copy(bf16[768,32]{1,0:T(8,128)(2,1)} %shard_map.208) | data formatting | bytes 98304 | tf_op jit(solution)/shard_map/pallas_call | solution.py:567
  (4 shorter events, 0.0 us)
Async XLA Ops:
  0.0 9.1 %copy-start = (bf16[4096,16]{0,1:T(8,128)(2,1)S(1)}, bf16[4096,16]{0,1:T(8,128)(2,1)}, u32[]{:S(2)}) copy-start(bf16[4096,16]{0,1:T(8,128)(2,1)} %param.29) | copy-start | bytes 393220

commit v2 on v1

--- a/solution.py
+++ b/solution.py
@@ -38,22 +38,24 @@
 
 def layer(
     tokens, norm_gain, w_query, w_key, w_value, w_outgate, w_igate, w_fgate, head_gain, w_proj,
-    mixer_gain, w_gate, w_up, w_down, state_c, tail_keys, tail_values, tail_gate, meta,
+    mixer_gain, w_gate, w_up, w_down, state_c, tail_keys, tail_values, tail_gate, state_m, block_forget,
+    lengths, forget_bias,
     out,
-    tok_v, wide_t, wide, scaled, wqkvo, wig_v, wfg_v, wproj_v, wgu, wdown_v, cbuf, kbuf, vbuf,
-    gsend, grecv,
+    wide_t, wide, scaled, wqkvo, wig_v, wfg_v, wproj_v, wgu, wdown_v, cbuf, kbuf, vbuf,
+    gsend, grecv, rows_v, tg_v,
     a_p, a_own, a_in, a_comb, a_l, a_r, a_q, a_qin, a_qcomb, a_ql, a_qr,
-    qs, tailo, mix_all, att_send, att_recv, mid_all, scaled_mid, ssend, srecv, mid_sel,
-    b_p, b_own, b_in, b_comb, b_l, b_r, b_q, b_qin, b_qcomb, b_ql, b_qr,
+    qs, mix_all, att_send, att_recv, mid_all, ssend, srecv, mid_sel,
+    lhs4, sm_own, b_own, b_q, b_qin, b_qcomb, b_ql, b_qr,
     hid, fsend, frecv,
     lsem, tok_s, tok_r, g_s, g_r, mix_s, mix_r, att_s, att_r, mid_s, mid_r, sq_s, sq_r,
-    ra_s, ra_r, rb_s, rb_r, h_s, h_r, f_s, f_r,
+    ra_s, ra_r, rb_s, rb_r, ws_s, ws_r, sm_s, sm_r, h_s, h_r, f_s, f_r,
 ):
     kv = lax.axis_index("kv")
     tp = lax.axis_index("tp")
     z = lax.div(kv, 4)
     x = lax.rem(kv, 4)
     c = lax.rem(tp, 2)
+    y = lax.div(tp, 2)
     pa = x * (1 - c) + z * c
     pb = z * (1 - c) + x * c
 
@@ -95,19 +97,19 @@
         sends.append(copy)
 
     loads = [
-        pltpu.make_async_copy(tokens, tok_v, lsem.at[0]),
+        pltpu.make_async_copy(tokens, wide_t.at[rows32(tp)], lsem.at[0]),
         pltpu.make_async_copy(w_query, wqkvo.at[:, pl.ds(0, 256)], lsem.at[1]),
         pltpu.make_async_copy(w_key, wqkvo.at[:, pl.ds(256, 256)], lsem.at[2]),
         pltpu.make_async_copy(w_value, wqkvo.at[:, pl.ds(512, 256)], lsem.at[3]),
         pltpu.make_async_copy(w_outgate, wqkvo.at[:, pl.ds(768, 256)], lsem.at[4]),
-        pltpu.make_async_copy(w_igate.at[pl.ds(pl.multiple_of(kv * 256, 256), 256)], wig_v, lsem.at[5]),
-        pltpu.make_async_copy(w_fgate.at[pl.ds(pl.multiple_of(kv * 256, 256), 256)], wfg_v, lsem.at[6]),
+        pltpu.make_async_copy(w_igate.at[:, pl.ds(pl.multiple_of(kv * 256, 256), 256)], wig_v, lsem.at[5]),
+        pltpu.make_async_copy(w_fgate.at[:, pl.ds(pl.multiple_of(kv * 256, 256), 256)], wfg_v, lsem.at[6]),
         pltpu.make_async_copy(state_c, cbuf, lsem.at[7]),
         pltpu.make_async_copy(tail_keys, kbuf, lsem.at[8]),
         pltpu.make_async_copy(tail_values, vbuf, lsem.at[9]),
         pltpu.make_async_copy(w_proj, wproj_v, lsem.at[10]),
-        pltpu.make_async_copy(w_gate, wgu.at[:, pl.ds(0, FFD)], lsem.at[11]),
-        pltpu.make_async_copy(w_up, wgu.at[:, pl.ds(FFD, FFD)], lsem.at[12]),
+        pltpu.make_async_copy(w_gate, wgu.at[pl.ds(0, 256), pl.ds(0, FFD)], lsem.at[11]),
+        pltpu.make_async_copy(w_up, wgu.at[pl.ds(0, 256), pl.ds(FFD, FFD)], lsem.at[12]),
         pltpu.make_async_copy(w_down, wdown_v, lsem.at[13]),
     ]
     for load in loads:
@@ -120,32 +122,59 @@
         pl.semaphore_signal(barrier, inc=1, device_id=(kv, tp_peer(r)), device_id_type=MESH)
 
     loads[0].wait()
-    tok_f = tok_v[...].astype(F32)
-    wide_t[rows32(tp), :] = tok_f.T.astype(BF)
     pl.semaphore_wait(barrier, 22)
 
     for r in range(1, 8):
         mine = wide_t.at[rows32(tp)]
         send(mine, mine, tok_s.at[r], tok_r.at[r], (kv, tp_peer(r)))
 
+    early, late = (0, 96), (96, 160)
+
+    def weight_rows(slot, part):
+        return wgu.at[pl.ds(256 * slot + part[0], part[1])]
+
+    def weight_send(src_slot, dst_slot, part, i, dev):
+        send(weight_rows(src_slot, part), weight_rows(dst_slot, part), ws_s.at[i], ws_r.at[i], dev)
+
+    def weight_wait(slot, part, i):
+        dst = weight_rows(slot, part)
+        remote(dst, dst, ws_s.at[i], ws_r.at[i], (kv, tp)).wait_recv()
+
+    loads[11].wait()
+    loads[12].wait()
+    weight_send(0, 1, early, 0, at_a(1))
+    weight_send(0, 3, early, 1, at_a(3))
     lane = lax.broadcasted_iota(jnp.int32, (128, 128), 1)
     for i in range(5, 7):
         loads[i].wait()
-    grow = lax.broadcasted_iota(jnp.int32, (16, 128), 0)
-    glane = lax.broadcasted_iota(jnp.int32, (16, 128), 1)
-    pick_i = jnp.where((glane < 2) & (grow == 2 * tp + glane), 1.0, 0.0).astype(BF)
-    pick_f = jnp.where((glane >= 2) & (glane < 4) & (grow == 2 * tp + glane - 2), 1.0, 0.0).astype(BF)
+    grow = lax.broadcasted_iota(jnp.int32, (128, 16), 0)
+    gcol = lax.broadcasted_iota(jnp.int32, (128, 16), 1)
+    pick_i = jnp.where((grow < 2) & (gcol == 2 * tp + grow), 1.0, 0.0).astype(BF)
+    pick_f = jnp.where((grow >= 2) & (grow < 4) & (gcol == 2 * tp + grow - 2), 1.0, 0.0).astype(BF)
     gate_w = (
-        jnp.dot(wig_v[...], pick_i, preferred_element_type=F32)
-        + jnp.dot(wfg_v[...], pick_f, preferred_element_type=F32)
-    ).astype(BF)
-    forget_row = meta[0:1, :]
-    state_row = meta[1:2, :]
-    length_row = meta[2:3, :]
-    bias_row = meta[3:4, :]
-    tg = transpose_padded(tail_gate[...])
+        jnp.dot(pick_i, wig_v[...], preferred_element_type=F32)
+        + jnp.dot(pick_f, wfg_v[...], preferred_element_type=F32)
+    ).T.astype(BF)
+    rows_v[...] = jnp.zeros((8, 128), F32)
+    rows_v[0:2, 0:48] = block_forget[...]
+    rows_v[2:4, 0:48] = state_m[...]
+    rows_v[4:5, 0:48] = lengths[...].astype(F32)
+    lane8 = lax.broadcasted_iota(jnp.int32, (8, 128), 1)
+
+    def pair_row(first, second):
+        a8 = jnp.broadcast_to(first, (8, 128))
+        b8 = jnp.broadcast_to(second, (8, 128))
+        return jnp.where(lane8 < 64, a8, pltpu.roll(b8, 64, 1))
+
+    forget_row = pair_row(rows_v[0:1, :], rows_v[1:2, :])
+    state_row = pair_row(rows_v[2:3, :], rows_v[3:4, :])
+    length_row = pair_row(rows_v[4:5, :], rows_v[4:5, :])[0:1]
+    bias_row = jnp.where(lane8 < 64, forget_bias[0], forget_bias[1])
+    tg_v[...] = jnp.zeros((128, 128), F32)
+    tg_v[0:48, 0:64] = tail_gate[:, 0, :]
+    tg_v[64:112, 0:64] = tail_gate[:, 1, :]
+    gate_t = tg_v[...].T[:64]
     lane64 = lax.broadcasted_iota(jnp.int32, (64, 128), 1)
-    gate_t = jnp.where(lane64 < 64, tg[:64], pltpu.roll(tg[64:], 64, 1))
 
     for r in range(1, 8):
         src = wide_t.at[rows32(tp_from(r))]
@@ -194,7 +223,6 @@
         send(p.at[1, :, second], from_l.at[:, second], ss.at[2], rs.at[2], right)
         group(3, into(p.at[2]))
         send(p.at[2, :, first], from_r.at[:, first], ss.at[3], rs.at[3], left)
-        group(0, into(own))
         between()
         waited(inn.at[0], 0)
 
@@ -210,6 +238,7 @@
 
         add_rows(192, comb1)
         send(comb.at[1], from_r.at[:, second], ss.at[5], rs.at[5], left)
+        group(0, into(own))
         waited(from_l.at[:, second], 2)
         waited(from_r.at[:, first], 3)
         waited(from_l.at[:, first], 4)
@@ -291,16 +320,11 @@
         scaled, wqkvo, N1, 256, a_p, a_own, a_in, a_comb, a_l, a_r, a_q, a_qin, a_qcomb, a_ql, a_qr,
         ra_s, ra_r, gate_tiles,
     )
+    weight_send(0, 1, late, 2, at_a(1))
+    weight_send(0, 3, late, 3, at_a(3))
     gsum = small_sum(grecv, gsend[kv], g_s, g_r)
     inv_row = lax.rsqrt(gsum[4:5, :] / D + EPS)
     inv_col = column_of(inv_row)[:48]
-    lane8 = lax.broadcasted_iota(jnp.int32, (8, 128), 1)
-
-    def pair_row(first, second):
-        a8 = jnp.broadcast_to(first, (8, 128))
-        b8 = jnp.broadcast_to(second, (8, 128))
-        return jnp.where(lane8 < 64, a8, pltpu.roll(b8, 64, 1))
-
     igate = pair_row(gsum[0:1, :] * inv_row, gsum[1:2, :] * inv_row)
     fpre = pair_row(gsum[2:3, :] * inv_row, gsum[3:4, :] * inv_row) + bias_row
     log_sig = -(jnp.maximum(-fpre, 0.0) + jnp.log1p(jnp.exp(-jnp.abs(fpre))))
@@ -318,29 +342,49 @@
     for i in range(7, 10):
         loads[i].wait()
 
+    pad16 = jnp.zeros((16, 128), F32)
+    q_t = jnp.concatenate([qs[0], pad16, qs[1], pad16], axis=0).T
+    q_hi = q_t.astype(BF)
+    q_lo = (q_t - q_hi.astype(F32)).astype(BF)
+    q_cols = jnp.concatenate([q_hi, q_lo], axis=1)
+    q_both = jnp.concatenate([q_cols, jnp.concatenate([q_hi, jnp.zeros((128, 128), BF)], axis=1)], axis=0)
+
     def recall_step(s, carry):
         mem_t, sc_t = carry
         for h in range(2):
-            qrow = qs[h, pl.ds(s, 1), :]
-            m = jnp.sum(cbuf[s, h] * qrow, axis=1, keepdims=True)
-            mem_t = jnp.where(lane == 64 * h + s, m, mem_t)
-            sc = jnp.sum(kbuf[s, h].astype(F32) * qrow, axis=1, keepdims=True)
-            sc_t = jnp.where(lane64 == 64 * h + s, sc, sc_t)
+            state = cbuf[s, h]
+            s_hi = state.astype(BF)
+            s_lo = (state - s_hi.astype(F32)).astype(BF)
+            m = jnp.dot(jnp.concatenate([s_hi, s_lo], axis=1), q_both, preferred_element_type=F32)
+            mem_t = jnp.where(lane == 64 * h + s, m[:, :128] + m[:, 128:], mem_t)
+            sc = jnp.dot(kbuf[s, h], q_cols, preferred_element_type=F32)
+            sc_t = jnp.where(lane64 == 64 * h + s, sc[:, :128] + sc[:, 128:], sc_t)
         return mem_t, sc_t
 
     mem_t, sc_t = lax.fori_loop(
-        0, 48, recall_step, (jnp.zeros((128, 128), F32), jnp.zeros((64, 128), F32))
+        0, 48, recall_step, (jnp.zeros((128, 128), F32), jnp.zeros((64, 128), F32)), unroll=2
     )
     weighted = w_tail * (sc_t * 128 ** (-0.5))
-
-    def tail_step(s, _):
-        for h in range(2):
-            wcol = jnp.sum(jnp.where(lane64 == 64 * h + s, weighted, 0.0), axis=1, keepdims=True)
-            tailo[h, pl.ds(s, 1), :] = jnp.sum(vbuf[s, h].astype(F32) * wcol, axis=0, keepdims=True)
-        return 0
-
-    lax.fori_loop(0, 48, tail_step, 0)
-    memory = (mem_t * w_inter).T
+    rows_w = jnp.concatenate([weighted, weighted], axis=0).T
+    prow = lax.broadcasted_iota(jnp.int32, (128, 256), 0)
+    plane = lax.broadcasted_iota(jnp.int32, (128, 256), 1)
+    slot = 2 * lax.rem(prow, 2) + lax.div(prow, 64)
+    rows_w = jnp.where(lax.div(plane, 64) == slot, jnp.concatenate([rows_w, rows_w], axis=1), 0.0)
+    w_hi = rows_w.astype(BF)
+    w_lo = (rows_w - w_hi.astype(F32)).astype(BF)
+    step_of = lax.div(lax.rem(prow, 64), 2)
+
+    def tail_step(g, acc):
+        here = jnp.where(step_of == g, 1.0, 0.0).astype(BF)
+        vals = vbuf[pl.ds(2 * g, 2)].reshape(256, 128)
+        return (
+            acc
+            + jnp.dot(w_hi * here, vals, preferred_element_type=F32)
+            + jnp.dot(w_lo * here, vals, preferred_element_type=F32)
+        )
+
+    tail_part = lax.fori_loop(0, 24, tail_step, jnp.zeros((128, 128), F32), unroll=2)
+    memory = (mem_t * w_inter).T + tail_part
     mixed = []
     for h in range(2):
         q = qs[h]
@@ -348,7 +392,7 @@
         v = proj(pl.ds(512 + 128 * h, 128)) * inv_col
         og = proj(pl.ds(768 + 128 * h, 128)) * inv_col
         own = jnp.sum(q * k, axis=1, keepdims=True)
-        recalled = memory[64 * h : 64 * h + 48] + tailo[h] + w_own[64 * h : 64 * h + 48] * own * v
+        recalled = memory[64 * h : 64 * h + 48] + w_own[64 * h : 64 * h + 48] * own * v
         ms = jnp.mean(recalled * recalled, axis=1, keepdims=True)
         normed = recalled * lax.rsqrt(ms + EPS)
         hg = head_gain[:, 128 * h : 128 * h + 128]
@@ -367,51 +411,152 @@
         att_send[r] = part.astype(BF)
         if r:
             send(att_send.at[r], att_recv.at[r], att_s.at[r], att_r.at[r], (kv, tp_peer(r)))
+    weight_wait(1, early, 0)
+    weight_wait(1, late, 2)
+    weight_send(1, 2, (0, 128), 4, at_a(1))
+    weight_wait(3, early, 1)
+    weight_wait(3, late, 3)
+    weight_send(3, 2, (128, 128), 5, at_a(3))
     attended = att_send[0].astype(F32)
     for r in range(1, 8):
         remote(att_recv.at[r], att_recv.at[r], att_s.at[r], att_r.at[r], (kv, tp)).wait_recv()
         attended = attended + att_recv[r].astype(F32)
-    mid_all[rows96(tp), :] = (wide[rows96(tp), :].astype(F32) + attended).astype(BF)
+    middle = (wide[rows96(tp), :].astype(F32) + attended).astype(BF)
+    mid_all[rows96(tp), :] = middle
+    middle_f = middle.astype(F32)
+    sm_block = (middle_f * mixer_gain[...]).astype(BF)
+    later = []
+
+    def send_unless(here, *args):
+        copy = remote(*args)
+
+        @pl.when(jnp.logical_not(here))
+        def _():
+            copy.start()
+
+        later.append((here, copy))
+
+    for i in range(2):
+        sm_own[i] = sm_block[48 * i : 48 * i + 48]
+    for n, (dy, dc, i) in enumerate((dy, dc, i) for dy in (2, 1, 3, 0) for dc in range(2) for i in range(2)):
+        k = 2 * tp + i
+        kz, kx = lax.div(k, 4), lax.rem(k, 4)
+        cd = lax.rem(c + dc, 2)
+        dev_kv = (1 - cd) * (4 * z + kx) + cd * (4 * kz + x)
+        ra = mod4((1 - cd) * (kx + 4 - x) + cd * (kz + 4 - z))
+        ib = (1 - cd) * kz + cd * kx
+        args = (
+            sm_own.at[i], lhs4.at[ra, rows48(ib)], sm_s.at[n], sm_r.at[ra * 4 + ib],
+            (dev_kv, 2 * mod4(y + dy) + cd),
+        )
+        if dy == 0 and dc == 0:
+            send_unless(dev_kv == kv, *args)
+        else:
+            send(*args)
+    for i in range(2):
+        sq = middle_f[48 * i : 48 * i + 48]
+        sq = sq * sq
+        row = jnp.sum(transpose_padded(sq[:, :128] + sq[:, 128:]), axis=0, keepdims=True)
+        ssend[i] = jnp.broadcast_to(row, (8, 128))
+        k = 2 * tp + i
+        slot = 4 * mod4(lax.div(k, 4) + 4 - z) + mod4(lax.rem(k, 4) + 4 - x)
+        for r in range(8):
+            args = (ssend.at[i], srecv.at[slot], sq_s.at[8 * i + r], sq_r.at[slot], (k, tp_peer(r)))
+            if r == 0:
+                send_unless(k == kv, *args)
+            else:
+                send(*args)
     for r in [4, 3, 5, 2, 6, 1, 7]:
         mine = mid_all.at[rows96(tp)]
         send(mine, mine, mid_s.at[r], mid_r.at[r], (kv, tp_peer(r)))
+
+    for n in (4, 5):
+        weight_wait(2, (128 * (n - 4), 128), n)
+    for ra in range(4):
+        for ib in range(4):
+            dst = lhs4.at[ra, pl.ds(48 * ib, 48)]
+            got = remote(dst, dst, sm_s.at[0], sm_r.at[ra * 4 + ib], (kv, tp))
+            if ra:
+                got.wait_recv()
+            else:
+                k = kv_of(pa, ib)
+                here = lax.div(k, 2) == tp
+
+                @pl.when(jnp.logical_not(here))
+                def _():
+                    got.wait_recv()
+
+                @pl.when(here)
+                def _():
+                    lhs4[0, 48 * ib : 48 * ib + 48, :] = sm_own[lax.rem(k, 2)]
+    rows_all = jnp.concatenate([lhs4[ra] for ra in range(4)], axis=1)
+    first, second = pl.ds(0, FFD), pl.ds(FFD, FFD)
+
+    def half_product(base):
+        def step(t, _):
+            cols = pl.ds(pl.multiple_of(base + t * 256, 128), 256)
+            b_own[:, cols] = jnp.dot(rows_all, wgu[:, cols], preferred_element_type=F32)
+            return 0
+
+        lax.fori_loop(0, 5, step, 0)
+        cols = pl.ds(base + 1280, 128)
+        b_own[:, cols] = jnp.dot(rows_all, wgu[:, cols], preferred_element_type=F32)
+
+    def b_rows(g):
+        return pl.ds(pl.multiple_of(mod4(pb + g) * 48, 16), 48)
+
+    def b_put(j, g, cols):
+        b_q[j, :, cols] = b_own[b_rows(g), cols].astype(BF)
+
+    def b_wait(dst, i):
+        remote(dst, dst, rb_s.at[i], rb_r.at[i], (kv, tp)).wait_recv()
+
+    right, left = at_b(1), at_b(3)
+    half_product(0)
+    b_put(0, 2, first)
+    send(b_q.at[0, :, first], b_qin.at[0], rb_s.at[6], rb_r.at[6], right)
+    b_put(2, 3, first)
+    send(b_q.at[2, :, first], b_qr.at[:, first], rb_s.at[9], rb_r.at[9], left)
+    half_product(FFD)
+    b_put(0, 2, second)
+    send(b_q.at[0, :, second], b_qin.at[1], rb_s.at[7], rb_r.at[7], left)
+    b_put(1, 1, second)
+    send(b_q.at[1, :, second], b_ql.at[:, second], rb_s.at[8], rb_r.at[8], right)
+    b_wait(b_qin.at[0], 6)
+    b_qcomb[0] = (b_own[b_rows(1), first] + b_qin[0].astype(F32)).astype(BF)
+    send(b_qcomb.at[0], b_ql.at[:, first], rb_s.at[10], rb_r.at[10], right)
+    b_wait(b_qin.at[1], 7)
+    b_qcomb[1] = (b_own[b_rows(3), second] + b_qin[1].astype(F32)).astype(BF)
+    send(b_qcomb.at[1], b_qr.at[:, second], rb_s.at[11], rb_r.at[11], left)
     for r in range(1, 8):
         src = mid_all.at[rows96(tp_from(r))]
         remote(src, src, mid_s.at[r], mid_r.at[r], (kv, tp)).wait_recv()
-
-    def scale_mid(k, _):
-        rows = rows48(k)
-        m = mid_all[rows, :].astype(F32)
-        scaled_mid[rows, :] = (m * mixer_gain[...]).astype(BF)
-        return 0
-
-    lax.fori_loop(0, 16, scale_mid, 0)
-
-    def square_tiles():
-        def step(k, _):
-            m = mid_all[rows48(k), :].astype(F32)
-            sq = m * m
-            row = jnp.sum(transpose_padded(sq[:, :128] + sq[:, 128:]), axis=0, keepdims=True)
-            ssend[k] = jnp.broadcast_to(row, (8, 128))
-            return 0
-
-        lax.fori_loop(0, 16, step, 0)
-        for i in range(1, 16):
-            k = kv_peer(i)
-            send(ssend.at[k], srecv.at[i], sq_s.at[i], sq_r.at[i], (k, tp))
-        srow = lax.broadcasted_iota(jnp.int32, (256, 128), 0)
-        slane = lax.broadcasted_iota(jnp.int32, (256, 128), 1)
-        pick = jnp.where((slane < 32) & (srow == 32 * tp + slane), 1.0, 0.0).astype(BF)
-        mid_sel[...] = jnp.dot(mid_all[...], pick, preferred_element_type=F32)
-
-    loads[11].wait()
-    loads[12].wait()
-    both = ring_sum(
-        scaled_mid, wgu, N2, 256, b_p, b_own, b_in, b_comb, b_l, b_r, b_q, b_qin, b_qcomb, b_ql, b_qr,
-        rb_s, rb_r, square_tiles,
+    srow = lax.broadcasted_iota(jnp.int32, (32, 256), 0)
+    scol = lax.broadcasted_iota(jnp.int32, (32, 256), 1)
+    pick = jnp.where(scol == 32 * tp + srow, 1.0, 0.0).astype(BF)
+    mid_sel[...] = lax.dot_general(
+        pick, mid_all[...], (((1,), (1,)), ((), ())), preferred_element_type=F32
     )
-    ssum = small_sum(srecv, ssend[kv], sq_s, sq_r)
+    sq_here = lax.div(kv, 2) == tp
+    sq0 = remote(srecv.at[0], srecv.at[0], sq_s.at[0], sq_r.at[0], (kv, tp))
+
+    @pl.when(jnp.logical_not(sq_here))
+    def _():
+        sq0.wait_recv()
+
+    @pl.when(sq_here)
+    def _():
+        srecv[0] = ssend[lax.rem(kv, 2)]
+
+    ssum = small_sum(srecv, srecv[0], sq_s, sq_r)
     inv_mid = column_of(lax.rsqrt(ssum[0:1] / D + EPS))[:48]
+    b_wait(b_ql.at[:, second], 8)
+    b_wait(b_qr.at[:, first], 9)
+    b_wait(b_ql.at[:, first], 10)
+    b_wait(b_qr.at[:, second], 11)
+
+    def both(cols):
+        return b_own[b_rows(0), cols] + b_ql[:, cols].astype(F32) + b_qr[:, cols].astype(F32)
 
     def hidden_step(t, _):
         cols = pl.ds(pl.multiple_of(t * 128, 128), 128)
@@ -478,12 +623,13 @@
     for r in range(1, 8):
         remote(frecv.at[r], frecv.at[r], f_s.at[r], f_r.at[r], (kv, tp)).wait_recv()
         total = total + frecv[r].astype(F32)
-    for b in range(6):
-        down = transpose_padded(total[:, 128 * b : 128 * b + 128])
-        rows = slice(128 * b, 128 * b + 128)
-        out[rows, :] = (mid_sel[rows, :] + down)[:, :32].astype(BF)
+    out[...] = (mid_sel[...] + total).astype(BF)
     for copy in sends:
         copy.wait_send()
+    for here, copy in later:
+        @pl.when(jnp.logical_not(here))
+        def _():
+            copy.wait_send()
 
 
 def per_device(
@@ -491,14 +637,6 @@
     w_proj, mixer_gain, w_gate, w_up, w_down, state_c, state_m, tail_keys, tail_values, tail_gate,
     block_forget, lengths,
 ):
-    def pair_row(a):
-        return jnp.pad(a.T, ((0, 0), (0, 16))).reshape(1, 128)
-
-    length_row = pair_row(jnp.broadcast_to(lengths.astype(F32)[:, None], (48, 2)))
-    bias_row = pair_row(jnp.broadcast_to(forget_bias[None, :], (48, 2)))
-    meta = jnp.concatenate(
-        [pair_row(block_forget), pair_row(state_m), length_row, bias_row, jnp.zeros((4, 128), F32)], axis=0
-    )
     any_spec = pl.BlockSpec(memory_space=pl.ANY)
     vm_spec = pl.BlockSpec(memory_space=pltpu.VMEM)
     dma = pltpu.SemaphoreType.DMA
@@ -519,33 +657,35 @@
         ]
 
     scratch = [
-        pltpu.VMEM((768, 32), BF),
         pltpu.VMEM((256, 768), BF),
         pltpu.VMEM((768, 256), BF),
         pltpu.VMEM((768, 256), BF),
         pltpu.VMEM((256, N1), BF),
-        pltpu.VMEM((256, 16), BF),
-        pltpu.VMEM((256, 16), BF),
+        pltpu.VMEM((16, 256), BF),
+        pltpu.VMEM((16, 256), BF),
         pltpu.VMEM((256, 256), BF),
-        pltpu.VMEM((256, N2), BF),
+        pltpu.VMEM((1024, N2), BF),
         pltpu.VMEM((FFD, 256), BF),
         pltpu.VMEM((48, 2, 128, 128), F32),
         pltpu.VMEM((48, 2, 64, 128), BF),
         pltpu.VMEM((48, 2, 64, 128), BF),
         pltpu.VMEM((16, 8, 128), F32),
         pltpu.VMEM((16, 8, 128), F32),
+        pltpu.VMEM((8, 128), F32),
+        pltpu.VMEM((128, 128), F32),
         *ring_bufs(N1),
-        pltpu.VMEM((2, 48, 128), F32),
         pltpu.VMEM((2, 48, 128), F32),
         pltpu.VMEM((768, 256), BF),
         pltpu.VMEM((8, 96, 256), BF),
         pltpu.VMEM((8, 96, 256), BF),
         pltpu.VMEM((768, 256), BF),
-        pltpu.VMEM((768, 256), BF),
+        pltpu.VMEM((2, 8, 128), F32),
         pltpu.VMEM((16, 8, 128), F32),
-        pltpu.VMEM((16, 8, 128), F32),
-        pltpu.VMEM((768, 128), F32),
-        *ring_bufs(N2),
+        pltpu.VMEM((32, 768), F32),
+        pltpu.VMEM((4, 192, 256), BF),
+        pltpu.VMEM((2, 48, 256), BF),
+        pltpu.VMEM((192, N2), F32),
+        *ring_bufs(N2)[6:],
         pltpu.VMEM((768, FFD), BF),
         pltpu.VMEM((256, 768), BF),
         pltpu.VMEM((8, 32, 768), BF),
@@ -558,15 +698,18 @@
         dma((16,)), dma((16,)),
         dma((12,)), dma((12,)),
         dma((12,)), dma((12,)),
+        dma((6,)), dma((6,)),
+        dma((16,)), dma((16,)),
         dma((16,)), dma((16,)),
         dma((8,)), dma((8,)),
     ]
-    specs = [any_spec] * 19
-    for i in (1, 8, 10, 17, 18):
+    specs = [any_spec] * 21
+    for i in (1, 8, 10, 17, 18, 19, 20):
         specs[i] = vm_spec
-    return pl.pallas_call(
+    specs.append(pl.BlockSpec(memory_space=pltpu.SMEM))
+    result_t = pl.pallas_call(
         layer,
-        out_shape=jax.ShapeDtypeStruct((768, 32), BF),
+        out_shape=jax.ShapeDtypeStruct((32, 768), BF),
         in_specs=specs,
         out_specs=vm_spec,
         scratch_shapes=scratch,
@@ -574,10 +717,11 @@
             collective_id=0, has_side_effects=True, vmem_limit_bytes=60 * 1024 * 1024
         ),
     )(
-        tokens, norm_gain.reshape(1, 256), w_query, w_key, w_value, w_outgate, w_igate, w_fgate,
+        tokens.T, norm_gain.reshape(1, 256), w_query, w_key, w_value, w_outgate, w_igate.T, w_fgate.T,
         head_gain.reshape(1, 256), w_proj, mixer_gain.reshape(1, 256), w_gate, w_up, w_down,
-        state_c, tail_keys, tail_values, tail_gate.reshape(48, 128), meta,
+        state_c, tail_keys, tail_values, tail_gate, state_m.T, block_forget.T, lengths.reshape(1, 48), forget_bias,
     )
+    return result_t.T
 
 
 def solution(mesh):

time: 135 us -> 110 us (0.81)
  Pallas kernels: 123 us -> 108 us
  local copies, waits for them, and re-layouts: 11.5 us -> 1.42 us
    pallas_call x1, Pallas kernels: 123 us -> 108 us  [per_device(): pl.pallas_call(layer, out_shape=jax.ShapeDtypeStruct((32, 768), BF), in_s...]
    unnamed x5 -> x1, local copies, waits for them, and re-layouts: 5.25 us -> 1.42 us
    reshape x5 -> x0, local copies, waits for them, and re-layouts: 1.84 us -> none  [the longest x1 1.5 us: per_device(): tail_gate.reshape(48, 128)]
    pallas_call x1 -> x0, local copies, waits for them, and re-layouts: 1.66 us -> none  [per_device(): pl.pallas_call(layer, out_shape=jax.ShapeDtypeStruct((768, 32), BF), in_s...]
    pad x5 -> x0, local copies, waits for them, and re-layouts: 1.38 us -> none  [pair_row(): return jnp.pad(a.T, ((0, 0), (0, 16))).reshape(1, 128)]
where the time goes in v2:
time: 110 us; the launch traced here: 109 us
  Pallas kernels  108 us (98%)
  local copies, waits for them, and re-layouts  1.42 us (1%)
    pallas_call x1, Pallas kernels, per_device(): pl.pallas_call(layer, out_shape=jax.ShapeDtypeStruct((32, 768), BF), in_s...  108 us

profile of v2, /device:TPU:1, one launch (start us, length us, event | category | flops | bytes accessed | tf_op | source)
XLA Modules:
  0.0 109.4 jit_solution(13094872543237165716)
XLA Ops:
  0.0 107.9 %shard_map.208 = bf16[32,768]{1,0:T(8,128)(2,1)} custom-call(bf16[32,768]{1,0:T(8,128)(2,1)} %bitcast.13, f32[1,256]{1,0:T(1,128)} %bitcast.14, bf16[256,256]{1,0:T(8,128)(2,1)} %w_query.1, bf16[256,256]{1,0:T(8,128)(2,1)} %w_key.1, bf16[256,256]{1,0:T(8,128)(2,1)} %w_value.1, bf16[256,256]{1,0:T(8,128)(2,1)} %w_outgate.1, bf16[16,4096]{1,0:T(8,128)(2,1)} %bitcast.11, ...), custom_call_target="tpu_custom_call" | custom-call | tf_op jit(solution)/shard_map/pallas_call | solution.py:710
  107.9 1.4 %copy.24 = bf16[768,32]{0,1:T(8,128)(2,1)} copy(bf16[768,32]{0,1:T(8,128)(2,1)} %bitcast.10) | data formatting | bytes 98304

commit v3 on v2

--- a/solution.py
+++ b/solution.py
@@ -44,11 +44,11 @@
     wide_t, wide, scaled, wqkvo, wig_v, wfg_v, wproj_v, wgu, wdown_v, cbuf, kbuf, vbuf,
     gsend, grecv, rows_v, tg_v,
     a_p, a_own, a_in, a_comb, a_l, a_r, a_q, a_qin, a_qcomb, a_ql, a_qr,
-    qs, mix_all, att_send, att_recv, mid_all, ssend, srecv, mid_sel,
+    qs, q_rows, mem_n, sc_n, mix_all, att_send, att_recv, mid_all, ssend, srecv, mid_sel,
     lhs4, sm_own, b_own, b_q, b_qin, b_qcomb, b_ql, b_qr,
-    hid, fsend, frecv,
+    hid, fsend, frecv, down_rows,
     lsem, tok_s, tok_r, g_s, g_r, mix_s, mix_r, att_s, att_r, mid_s, mid_r, sq_s, sq_r,
-    ra_s, ra_r, rb_s, rb_r, ws_s, ws_r, sm_s, sm_r, h_s, h_r, f_s, f_r,
+    ra_s, ra_r, rb_s, rb_r, ws_s, ws_r, sm_s, sm_r, wd_s, wd_r, h_s, h_r, f_s, f_r,
 ):
     kv = lax.axis_index("kv")
     tp = lax.axis_index("tp")
@@ -110,7 +110,7 @@
         pltpu.make_async_copy(w_proj, wproj_v, lsem.at[10]),
         pltpu.make_async_copy(w_gate, wgu.at[pl.ds(0, 256), pl.ds(0, FFD)], lsem.at[11]),
         pltpu.make_async_copy(w_up, wgu.at[pl.ds(0, 256), pl.ds(FFD, FFD)], lsem.at[12]),
-        pltpu.make_async_copy(w_down, wdown_v, lsem.at[13]),
+        pltpu.make_async_copy(w_down, wdown_v.at[:, pl.ds(0, 256)], lsem.at[13]),
     ]
     for load in loads:
         load.start()
@@ -197,7 +197,7 @@
                 put(cols, jnp.dot(rows, weights[:, cols], preferred_element_type=F32))
                 return 0
 
-            lax.fori_loop(0, n // tile, step, 0)
+            lax.fori_loop(0, n // tile, step, 0, unroll=True)
 
         def into(ref):
             def put(cols, value):
@@ -264,6 +264,8 @@
         total(2, into_q(0))
         send(q.at[0, :, first], qin.at[0], ss.at[6], rs.at[6], right)
         send(q.at[0, :, second], qin.at[1], ss.at[7], rs.at[7], left)
+        weight_send(0, 1, late, 2, at_a(1))
+        weight_send(0, 3, late, 3, at_a(3))
         total(1, into_q(1))
         send(q.at[1, :, second], ql.at[:, second], ss.at[8], rs.at[8], right)
         total(3, into_q(2))
@@ -309,7 +311,7 @@
             gsend[k] = transpose_padded(jnp.where(lane48 == 4, sq, part))[:8]
             return 0
 
-        lax.fori_loop(0, 16, step, 0)
+        lax.fori_loop(0, 16, step, 0, unroll=4)
         for i in range(1, 16):
             k = kv_peer(i)
             send(gsend.at[k], grecv.at[i], g_s.at[i], g_r.at[i], (k, tp))
@@ -320,8 +322,6 @@
         scaled, wqkvo, N1, 256, a_p, a_own, a_in, a_comb, a_l, a_r, a_q, a_qin, a_qcomb, a_ql, a_qr,
         ra_s, ra_r, gate_tiles,
     )
-    weight_send(0, 1, late, 2, at_a(1))
-    weight_send(0, 3, late, 3, at_a(3))
     gsum = small_sum(grecv, gsend[kv], g_s, g_r)
     inv_row = lax.rsqrt(gsum[4:5, :] / D + EPS)
     inv_col = column_of(inv_row)[:48]
@@ -342,28 +342,35 @@
     for i in range(7, 10):
         loads[i].wait()
 
-    pad16 = jnp.zeros((16, 128), F32)
-    q_t = jnp.concatenate([qs[0], pad16, qs[1], pad16], axis=0).T
-    q_hi = q_t.astype(BF)
-    q_lo = (q_t - q_hi.astype(F32)).astype(BF)
-    q_cols = jnp.concatenate([q_hi, q_lo], axis=1)
-    q_both = jnp.concatenate([q_cols, jnp.concatenate([q_hi, jnp.zeros((128, 128), BF)], axis=1)], axis=0)
-
-    def recall_step(s, carry):
-        mem_t, sc_t = carry
-        for h in range(2):
-            state = cbuf[s, h]
-            s_hi = state.astype(BF)
-            s_lo = (state - s_hi.astype(F32)).astype(BF)
-            m = jnp.dot(jnp.concatenate([s_hi, s_lo], axis=1), q_both, preferred_element_type=F32)
-            mem_t = jnp.where(lane == 64 * h + s, m[:, :128] + m[:, 128:], mem_t)
-            sc = jnp.dot(kbuf[s, h], q_cols, preferred_element_type=F32)
-            sc_t = jnp.where(lane64 == 64 * h + s, sc[:, :128] + sc[:, 128:], sc_t)
-        return mem_t, sc_t
-
-    mem_t, sc_t = lax.fori_loop(
-        0, 48, recall_step, (jnp.zeros((128, 128), F32), jnp.zeros((64, 128), F32)), unroll=2
-    )
+    for h in range(2):
+        q_hi = qs[h].astype(BF).astype(F32)
+        q_lo = (qs[h] - q_hi).astype(BF).astype(F32)
+        q_rows[:, 2 * h, :] = jnp.concatenate([q_hi, q_hi], axis=1)
+        q_rows[:, 2 * h + 1, :] = jnp.concatenate([q_lo, jnp.zeros((48, 128), F32)], axis=1)
+    for i in range(4, 8):
+        q_rows[:, i, :] = jnp.zeros((48, 256), F32)
+    contract_last = (((1,), (1,)), ((), ()))
+    lane1 = lax.broadcasted_iota(jnp.int32, (1, 128), 1)
+
+    def recall_step(s, _):
+        lhs = q_rows[s].astype(BF)
+        state = cbuf[s].reshape(256, 128)
+        s_hi = state.astype(BF)
+        s_lo = (state - s_hi.astype(F32)).astype(BF)
+        m = lax.dot_general(
+            lhs, jnp.concatenate([s_hi, s_lo], axis=1), contract_last, preferred_element_type=F32
+        )
+        mem_n[0, pl.ds(s, 1), :] = m[0:1, :128] + m[1:2, :128]
+        mem_n[1, pl.ds(s, 1), :] = m[2:3, 128:] + m[3:4, 128:]
+        sc = lax.dot_general(
+            lhs[:, :128], kbuf[s].reshape(128, 128), contract_last, preferred_element_type=F32
+        )
+        sc_n[pl.ds(s, 1), :] = jnp.where(lane1 < 64, sc[0:1] + sc[1:2], sc[2:3] + sc[3:4])
+        return 0
+
+    lax.fori_loop(0, 48, recall_step, 0, unroll=4)
+    sc_r = transpose_padded(sc_n[...])
+    sc_t = jnp.where(lane64 < 64, sc_r[:64], pltpu.roll(sc_r[64:], 64, 1))
     weighted = w_tail * (sc_t * 128 ** (-0.5))
     rows_w = jnp.concatenate([weighted, weighted], axis=0).T
     prow = lax.broadcasted_iota(jnp.int32, (128, 256), 0)
@@ -383,8 +390,8 @@
             + jnp.dot(w_lo * here, vals, preferred_element_type=F32)
         )
 
-    tail_part = lax.fori_loop(0, 24, tail_step, jnp.zeros((128, 128), F32), unroll=2)
-    memory = (mem_t * w_inter).T + tail_part
+    tail_part = lax.fori_loop(0, 24, tail_step, jnp.zeros((128, 128), F32), unroll=4)
+    w_state = column_of(w_inter)
     mixed = []
     for h in range(2):
         q = qs[h]
@@ -392,7 +399,8 @@
         v = proj(pl.ds(512 + 128 * h, 128)) * inv_col
         og = proj(pl.ds(768 + 128 * h, 128)) * inv_col
         own = jnp.sum(q * k, axis=1, keepdims=True)
-        recalled = memory[64 * h : 64 * h + 48] + w_own[64 * h : 64 * h + 48] * own * v
+        rows = slice(64 * h, 64 * h + 48)
+        recalled = mem_n[h] * w_state[rows] + tail_part[rows] + w_own[rows] * own * v
         ms = jnp.mean(recalled * recalled, axis=1, keepdims=True)
         normed = recalled * lax.rsqrt(ms + EPS)
         hg = head_gain[:, 128 * h : 128 * h + 128]
@@ -406,17 +414,17 @@
         src = mix_all.at[rows48(kv_from(i))]
         remote(src, src, mix_s.at[i], mix_r.at[i], (kv, tp)).wait_recv()
 
-    for r in [4, 3, 5, 2, 6, 1, 7, 0]:
-        part = jnp.dot(mix_all[rows96(tp_peer(r)), :], wproj_v[...], preferred_element_type=F32)
-        att_send[r] = part.astype(BF)
-        if r:
-            send(att_send.at[r], att_recv.at[r], att_s.at[r], att_r.at[r], (kv, tp_peer(r)))
     weight_wait(1, early, 0)
     weight_wait(1, late, 2)
     weight_send(1, 2, (0, 128), 4, at_a(1))
     weight_wait(3, early, 1)
     weight_wait(3, late, 3)
     weight_send(3, 2, (128, 128), 5, at_a(3))
+    for r in [4, 3, 5, 2, 6, 1, 7, 0]:
+        part = jnp.dot(mix_all[rows96(tp_peer(r)), :], wproj_v[...], preferred_element_type=F32)
+        att_send[r] = part.astype(BF)
+        if r:
+            send(att_send.at[r], att_recv.at[r], att_s.at[r], att_r.at[r], (kv, tp_peer(r)))
     attended = att_send[0].astype(F32)
     for r in range(1, 8):
         remote(att_recv.at[r], att_recv.at[r], att_s.at[r], att_r.at[r], (kv, tp)).wait_recv()
@@ -466,6 +474,20 @@
                 send_unless(k == kv, *args)
             else:
                 send(*args)
+    def down_weights(slot, part=(0, FFD)):
+        return wdown_v.at[pl.ds(part[0], part[1]), pl.ds(256 * slot, 256)]
+
+    def down_send(src_slot, dst_slot, part, i, dev):
+        send(down_weights(src_slot, part), down_weights(dst_slot, part), wd_s.at[i], wd_r.at[i], dev)
+
+    def down_got(slot, part, i):
+        dst = down_weights(slot, part)
+        remote(dst, dst, wd_s.at[i], wd_r.at[i], (kv, tp)).wait_recv()
+
+    whole, upper, lower = (0, FFD), (0, FFD // 2), (FFD // 2, FFD // 2)
+    loads[13].wait()
+    down_send(0, 1, whole, 0, at_a(1))
+    down_send(0, 3, whole, 1, at_a(3))
     for r in [4, 3, 5, 2, 6, 1, 7]:
         mine = mid_all.at[rows96(tp)]
         send(mine, mine, mid_s.at[r], mid_r.at[r], (kv, tp_peer(r)))
@@ -498,7 +520,7 @@
             b_own[:, cols] = jnp.dot(rows_all, wgu[:, cols], preferred_element_type=F32)
             return 0
 
-        lax.fori_loop(0, 5, step, 0)
+        lax.fori_loop(0, 5, step, 0, unroll=True)
         cols = pl.ds(base + 1280, 128)
         b_own[:, cols] = jnp.dot(rows_all, wgu[:, cols], preferred_element_type=F32)
 
@@ -528,6 +550,10 @@
     b_wait(b_qin.at[1], 7)
     b_qcomb[1] = (b_own[b_rows(3), second] + b_qin[1].astype(F32)).astype(BF)
     send(b_qcomb.at[1], b_qr.at[:, second], rb_s.at[11], rb_r.at[11], left)
+    down_got(1, whole, 0)
+    down_send(1, 2, upper, 2, at_a(1))
+    down_got(3, whole, 1)
+    down_send(3, 2, lower, 3, at_a(3))
     for r in range(1, 8):
         src = mid_all.at[rows96(tp_from(r))]
         remote(src, src, mid_s.at[r], mid_r.at[r], (kv, tp)).wait_recv()
@@ -562,18 +588,13 @@
         cols = pl.ds(pl.multiple_of(t * 128, 128), 128)
         gate = both(cols) * inv_mid
         up = both(pl.ds(pl.multiple_of(t * 128 + FFD, 128), 128)) * inv_mid
-        hid[rows48(kv), cols] = (gate * (1.0 / (1.0 + jnp.exp(-gate))) * up).astype(BF)
+        hid[rows48(pb), cols] = (gate * (1.0 / (1.0 + jnp.exp(-gate))) * up).astype(BF)
         return 0
 
     lax.fori_loop(0, FFD // 128, hidden_step, 0)
 
-    part_rows = (pl.ds(0, 32), pl.ds(32, 16))
-
-    def chunk(ra, rb):
-        return hid.at[rows48(kv_of(mod4(pa + 4 - ra), mod4(pb + 4 - rb)))]
-
-    def piece(ref, i):
-        return ref.at[part_rows[i]]
+    def chunk(rb, part=(0, 48)):
+        return hid.at[pl.ds(pl.multiple_of(mod4(pb + 4 - rb) * 48 + part[0], 16), part[1])]
 
     def hop(ref, i, dev):
         send(ref, ref, h_s.at[i], h_r.at[i], dev)
@@ -581,49 +602,62 @@
     def arrived(ref, i):
         remote(ref, ref, h_s.at[i], h_r.at[i], (kv, tp)).wait_recv()
 
-    def spread(rb):
-        hop(chunk(0, rb), 4 + rb, at_a(1))
-        hop(chunk(0, rb), 8 + rb, at_a(3))
-
-    hop(chunk(0, 0), 0, at_b(1))
-    hop(chunk(0, 0), 1, at_b(3))
-    spread(0)
-    arrived(chunk(0, 1), 0)
-    hop(piece(chunk(0, 1), 0), 2, at_b(1))
-    spread(1)
-    arrived(chunk(0, 3), 1)
-    hop(piece(chunk(0, 3), 1), 3, at_b(3))
-    spread(3)
-    arrived(chunk(1, 0), 4)
-    hop(chunk(1, 0), 12, at_a(1))
-    arrived(piece(chunk(0, 2), 0), 2)
-    arrived(piece(chunk(0, 2), 1), 3)
-    spread(2)
-    arrived(chunk(1, 1), 5)
-    hop(chunk(1, 1), 13, at_a(1))
-    arrived(chunk(3, 3), 11)
-    hop(chunk(3, 3), 15, at_a(3))
-    arrived(chunk(3, 2), 10)
-    hop(chunk(3, 2), 14, at_a(3))
-    loads[13].wait()
-    arrived(chunk(1, 2), 6)
-    arrived(chunk(1, 3), 7)
-    arrived(chunk(3, 0), 8)
-    arrived(chunk(3, 1), 9)
-    for rb in range(4):
-        arrived(chunk(2, rb), 12 + rb)
-
+    hop(chunk(0), 0, at_b(1))
+    hop(chunk(0), 1, at_b(3))
+    arrived(chunk(1), 0)
+    hop(chunk(1, (0, 32)), 2, at_b(1))
+    arrived(chunk(3), 1)
+    hop(chunk(3, (32, 16)), 3, at_b(3))
+    down_got(2, upper, 2)
+    down_got(2, lower, 3)
+    arrived(chunk(2, (0, 32)), 2)
+    arrived(chunk(2, (32, 16)), 3)
+
+    lane16 = lax.broadcasted_iota(jnp.int32, (8, 16, 128), 2)
+    for ra in (2, 1, 3, 0):
+        part = jnp.dot(hid[...], wdown_v[:, 256 * ra : 256 * ra + 256], preferred_element_type=F32)
+        part = jnp.concatenate([part, jnp.zeros((64, 256), F32)], axis=0).T
+        tail = part[:, 128:].reshape(8, 2, 16, 128)
+        tail = jnp.where(lane16 < 64, tail[:, 0], pltpu.roll(tail[:, 1], 64, 2))
+        fsend[ra, :, 0:32, :] = part[:, :128].reshape(8, 32, 128).astype(BF)
+        fsend[ra, :, 32:48, :] = tail.astype(BF)
+        for dy in (2, 1, 3, 0):
+            for dc in range(2):
+                t = 2 * mod4(y + dy) + lax.rem(c + dc, 2)
+                if ra or dy or dc:
+                    send(
+                        fsend.at[ra, t], frecv.at[c, ra, dy], f_s.at[8 * ra + 2 * dy + dc],
+                        f_r.at[16 * c + 4 * ra + dy], (kv_of(mod4(pa + 4 - ra), pb), t),
+                    )
+    frecv[c, 0, 0] = fsend[0, tp]
+    other = frecv.at[1 - c, 0, 0]
+    remote(other, other, f_s.at[0], f_r.at[16 * (1 - c)], (kv, tp)).wait_recv()
+    for cs in range(2):
+        mains, tails = [], []
+        for ra in range(4):
+            piece = 0.0
+            for dy in range(4):
+                dst = frecv.at[cs, ra, dy]
+                if ra or dy:
+                    remote(dst, dst, f_s.at[0], f_r.at[16 * cs + 4 * ra + dy], (kv, tp)).wait_recv()
+                piece = piece + frecv[cs, ra, dy].astype(F32)
+            mains.append(piece[:32])
+            tails += [piece[32:], pltpu.roll(piece[32:], 64, 1)]
+        by_seq = jnp.concatenate(
+            [jnp.concatenate(mains, axis=0).T, jnp.concatenate(tails, axis=0).T[:64]], axis=0
+        )
+        for ra in range(4):
+            block = pltpu.roll(by_seq, (128 - 32 * ra) % 128, 1) if ra else by_seq
+            for ib in range(4):
+                k = 4 * ib + mod4(x + ra) if cs == 0 else 4 * mod4(z + ra) + ib
+                mine = block[48 * ib : 48 * ib + 48]
+                if cs == 0:
+                    down_rows[rows48(k), :] = mine
+                else:
+                    down_rows[rows48(k), :] += mine
     for b in range(6):
-        part = jnp.dot(hid[128 * b : 128 * b + 128, :], wdown_v[...], preferred_element_type=F32)
-        fsend[:, 128 * b : 128 * b + 128] = part.T.astype(BF)
-    for r in [4, 3, 5, 2, 6, 1, 7]:
-        t = tp_peer(r)
-        send(fsend.at[rows32(t)], frecv.at[r], f_s.at[r], f_r.at[r], (kv, t))
-    total = fsend[rows32(tp), :].astype(F32)
-    for r in range(1, 8):
-        remote(frecv.at[r], frecv.at[r], f_s.at[r], f_r.at[r], (kv, tp)).wait_recv()
-        total = total + frecv[r].astype(F32)
-    out[...] = (mid_sel[...] + total).astype(BF)
+        cols = slice(128 * b, 128 * b + 128)
+        out[:, cols] = (mid_sel[:, cols] + down_rows[cols, :].T[:32]).astype(BF)
     for copy in sends:
         copy.wait_send()
     for here, copy in later:
@@ -665,7 +699,7 @@
         pltpu.VMEM((16, 256), BF),
         pltpu.VMEM((256, 256), BF),
         pltpu.VMEM((1024, N2), BF),
-        pltpu.VMEM((FFD, 256), BF),
+        pltpu.VMEM((FFD, 1024), BF),
         pltpu.VMEM((48, 2, 128, 128), F32),
         pltpu.VMEM((48, 2, 64, 128), BF),
         pltpu.VMEM((48, 2, 64, 128), BF),
@@ -675,6 +709,9 @@
         pltpu.VMEM((128, 128), F32),
         *ring_bufs(N1),
         pltpu.VMEM((2, 48, 128), F32),
+        pltpu.VMEM((48, 8, 256), F32),
+        pltpu.VMEM((2, 48, 128), F32),
+        pltpu.VMEM((48, 128), F32),
         pltpu.VMEM((768, 256), BF),
         pltpu.VMEM((8, 96, 256), BF),
         pltpu.VMEM((8, 96, 256), BF),
@@ -686,9 +723,10 @@
         pltpu.VMEM((2, 48, 256), BF),
         pltpu.VMEM((192, N2), F32),
         *ring_bufs(N2)[6:],
-        pltpu.VMEM((768, FFD), BF),
-        pltpu.VMEM((256, 768), BF),
-        pltpu.VMEM((8, 32, 768), BF),
+        pltpu.VMEM((192, FFD), BF),
+        pltpu.VMEM((4, 8, 48, 128), BF),
+        pltpu.VMEM((2, 4, 4, 48, 128), BF),
+        pltpu.VMEM((768, 128), F32),
         dma((14,)),
         dma((8,)), dma((8,)),
         dma((16,)), dma((16,)),
@@ -700,8 +738,9 @@
         dma((12,)), dma((12,)),
         dma((6,)), dma((6,)),
         dma((16,)), dma((16,)),
-        dma((16,)), dma((16,)),
-        dma((8,)), dma((8,)),
+        dma((4,)), dma((4,)),
+        dma((4,)), dma((4,)),
+        dma((32,)), dma((32,)),
     ]
     specs = [any_spec] * 21
     for i in (1, 8, 10, 17, 18, 19, 20):

time: 110 us -> 97.4 us (0.89)
  Pallas kernels: 108 us -> 95.8 us
    pallas_call x1, Pallas kernels: 108 us -> 95.8 us  [per_device(): pl.pallas_call(layer, out_shape=jax.ShapeDtypeStruct((32, 768), BF), in_s...]
where the time goes in v3:
time: 97.4 us; the launch traced here: 97.2 us
  Pallas kernels  95.8 us (98%)
  local copies, waits for them, and re-layouts  1.42 us (1%)
    pallas_call x1, Pallas kernels, per_device(): pl.pallas_call(layer, out_shape=jax.ShapeDtypeStruct((32, 768), BF), in_s...  95.8 us

profile of v3, /device:TPU:1, one launch (start us, length us, event | category | flops | bytes accessed | tf_op | source)
XLA Modules:
  0.0 97.2 jit_solution(358978194505138835)
XLA Ops:
  0.0 95.8 %shard_map.208 = bf16[32,768]{1,0:T(8,128)(2,1)} custom-call(bf16[32,768]{1,0:T(8,128)(2,1)} %bitcast.13, f32[1,256]{1,0:T(1,128)} %bitcast.14, bf16[256,256]{1,0:T(8,128)(2,1)} %w_query.1, bf16[256,256]{1,0:T(8,128)(2,1)} %w_key.1, bf16[256,256]{1,0:T(8,128)(2,1)} %w_value.1, bf16[256,256]{1,0:T(8,128)(2,1)} %w_outgate.1, bf16[16,4096]{1,0:T(8,128)(2,1)} %bitcast.11, ...), custom_call_target="tpu_custom_call" | custom-call | tf_op jit(solution)/shard_map/pallas_call | solution.py:749
  95.8 1.4 %copy.24 = bf16[768,32]{0,1:T(8,128)(2,1)} copy(bf16[768,32]{0,1:T(8,128)(2,1)} %bitcast.10) | data formatting | bytes 98304

commit v4 on v3

--- a/solution.py
+++ b/solution.py
@@ -11,6 +11,7 @@
 BF = jnp.bfloat16
 MESH = pl.DeviceIdType.MESH
 N1 = 1024
+NH = 512
 N2 = 2816
 FFD = 1408
 
@@ -43,13 +44,16 @@
     out,
     wide_t, wide, scaled, wqkvo, wig_v, wfg_v, wproj_v, wgu, wdown_v, cbuf, kbuf, vbuf,
     gsend, grecv, rows_v, tg_v,
-    a_p, a_own, a_in, a_comb, a_l, a_r, a_q, a_qin, a_qcomb, a_ql, a_qr,
-    qs, q_rows, mem_n, sc_n, mix_all, att_send, att_recv, mid_all, ssend, srecv, mid_sel,
-    lhs4, sm_own, b_own, b_q, b_qin, b_qcomb, b_ql, b_qr,
-    hid, fsend, frecv, down_rows,
-    lsem, tok_s, tok_r, g_s, g_r, mix_s, mix_r, att_s, att_r, mid_s, mid_r, sq_s, sq_r,
-    ra_s, ra_r, rb_s, rb_r, ws_s, ws_r, sm_s, sm_r, wd_s, wd_r, h_s, h_r, f_s, f_r,
+    *rest,
 ):
+    qk_bufs, vo_bufs, rest = rest[:13], rest[13:26], rest[26:]
+    (
+        qs, q_rows, mem_n, sc_n, mix_all, att_send, att_recv, mid_all, ssend, srecv, mid_sel,
+        lhs4, sm_own, b_own, b_q, b_qin, b_qcomb, b_ql, b_qr,
+        hid, fsend, frecv, down_rows,
+        lsem, tok_s, tok_r, g_s, g_r, mix_s, mix_r, att_s, att_r, mid_s, mid_r, sq_s, sq_r,
+        qk_s, qk_r, vo_s, vo_r, rb_s, rb_r, ws_s, ws_r, sm_s, sm_r, wd_s, wd_r, h_s, h_r, f_s, f_r,
+    ) = rest
     kv = lax.axis_index("kv")
     tp = lax.axis_index("tp")
     z = lax.div(kv, 4)
@@ -184,114 +188,98 @@
         wide[128 * b : 128 * b + 128, :] = block.astype(BF)
         scaled[128 * b : 128 * b + 128, :] = (block * norm_gain[...]).astype(BF)
 
-    def ring_sum(lhs, weights, n, tile, p, own, inn, comb, from_l, from_r, q, qin, qcomb, ql, qr, ss, rs, between):
-        half = n // 2
+    def ring(base, p, own, inn, comb, from_l, from_r, q, qin, qcomb, ql, qr, p_wide, q_wide, ss, rs):
+        half = NH // 2
         first, second = pl.ds(0, half), pl.ds(half, half)
 
-        def group(g, put):
+        def group(g, *outs):
             ia = mod4(pa + g)
-            rows = jnp.concatenate([lhs[rows48(kv_of(ia, ib)), :] for ib in range(4)], axis=0)
-
-            def step(t, _):
-                cols = pl.ds(pl.multiple_of(t * tile, tile), tile)
-                put(cols, jnp.dot(rows, weights[:, cols], preferred_element_type=F32))
-                return 0
-
-            lax.fori_loop(0, n // tile, step, 0, unroll=True)
-
-        def into(ref):
-            def put(cols, value):
-                ref[:, cols] = value.astype(ref.dtype)
-
-            return put
-
-        def add_rows(count, fn):
-            def step(i, _):
-                fn(pl.ds(pl.multiple_of(i * 16, 16), 16))
-                return 0
-
-            lax.fori_loop(0, count // 16, step, 0)
+            rows = jnp.concatenate([scaled[rows48(kv_of(ia, ib)), :] for ib in range(4)], axis=0)
+            for t, out_ref in enumerate(outs):
+                value = jnp.dot(
+                    rows, wqkvo[:, base + half * t : base + half * t + half], preferred_element_type=F32
+                )
+                out_ref[...] = value.astype(out_ref.dtype)
 
         def waited(dst, i):
             remote(dst, dst, ss.at[i], rs.at[i], (kv, tp)).wait_recv()
 
-        right, left = at_a(1), at_a(3)
-        group(2, into(p.at[0]))
-        send(p.at[0, :, first], inn.at[0], ss.at[0], rs.at[0], right)
-        send(p.at[0, :, second], inn.at[1], ss.at[1], rs.at[1], left)
-        group(1, into(p.at[1]))
-        send(p.at[1, :, second], from_l.at[:, second], ss.at[2], rs.at[2], right)
-        group(3, into(p.at[2]))
-        send(p.at[2, :, first], from_r.at[:, first], ss.at[3], rs.at[3], left)
-        between()
-        waited(inn.at[0], 0)
-
-        def comb0(rows):
-            comb[0, rows, :] = (p[1, rows, first].astype(F32) + inn[0, rows, :].astype(F32)).astype(BF)
-
-        add_rows(192, comb0)
-        send(comb.at[0], from_l.at[:, first], ss.at[4], rs.at[4], right)
-        waited(inn.at[1], 1)
-
-        def comb1(rows):
-            comb[1, rows, :] = (p[2, rows, second].astype(F32) + inn[1, rows, :].astype(F32)).astype(BF)
-
-        add_rows(192, comb1)
-        send(comb.at[1], from_r.at[:, second], ss.at[5], rs.at[5], left)
-        group(0, into(own))
-        waited(from_l.at[:, second], 2)
-        waited(from_r.at[:, first], 3)
-        waited(from_l.at[:, first], 4)
-        waited(from_r.at[:, second], 5)
-
-        right, left = at_b(1), at_b(3)
-
         def total(g, put):
-            base = mod4(pb + g) * 48
+            start = mod4(pb + g) * 48
             for i in range(3):
-                rows = pl.ds(pl.multiple_of(base + 16 * i, 16), 16)
+                rows = pl.ds(pl.multiple_of(start + 16 * i, 16), 16)
                 put(
                     pl.ds(16 * i, 16),
                     own[rows, :] + from_l[rows, :].astype(F32) + from_r[rows, :].astype(F32),
                 )
 
-        def into_q(j):
+        def into_q(j, i=None):
             def put(rows, value):
                 q[j, rows, :] = value.astype(BF)
+                if i is not None:
+                    q_wide[i, rows, :] = value[:, half * i : half * i + half]
 
             return put
 
-        total(2, into_q(0))
-        send(q.at[0, :, first], qin.at[0], ss.at[6], rs.at[6], right)
-        send(q.at[0, :, second], qin.at[1], ss.at[7], rs.at[7], left)
-        weight_send(0, 1, late, 2, at_a(1))
-        weight_send(0, 3, late, 3, at_a(3))
-        total(1, into_q(1))
-        send(q.at[1, :, second], ql.at[:, second], ss.at[8], rs.at[8], right)
-        total(3, into_q(2))
-        send(q.at[2, :, first], qr.at[:, first], ss.at[9], rs.at[9], left)
-        waited(qin.at[0], 6)
-        qcomb[0] = (q[1, :, first].astype(F32) + qin[0].astype(F32)).astype(BF)
-        send(qcomb.at[0], ql.at[:, first], ss.at[10], rs.at[10], right)
-        waited(qin.at[1], 7)
-        qcomb[1] = (q[2, :, second].astype(F32) + qin[1].astype(F32)).astype(BF)
-        send(qcomb.at[1], qr.at[:, second], ss.at[11], rs.at[11], left)
-        mine = pl.ds(pl.multiple_of(pb * 48, 16), 48)
-        waited(ql.at[:, second], 8)
-        waited(qr.at[:, first], 9)
-        waited(ql.at[:, first], 10)
-        waited(qr.at[:, second], 11)
-
-        def result(cols):
-            return (
-                own[mine, cols]
-                + from_l[mine, cols].astype(F32)
-                + from_r[mine, cols].astype(F32)
-                + ql[:, cols].astype(F32)
-                + qr[:, cols].astype(F32)
-            )
-
-        return result
+        class Stages:
+            def opposite(self):
+                group(2, p.at[0, :, first], p.at[0, :, second])
+                send(p.at[0, :, first], inn.at[0], ss.at[0], rs.at[0], at_a(1))
+                send(p.at[0, :, second], inn.at[1], ss.at[1], rs.at[1], at_a(3))
+
+            def plain(self):
+                group(1, p_wide.at[0], p.at[1, :, second])
+                send(p.at[1, :, second], from_l.at[:, second], ss.at[2], rs.at[2], at_a(1))
+                group(3, p.at[2, :, first], p_wide.at[1])
+                send(p.at[2, :, first], from_r.at[:, first], ss.at[3], rs.at[3], at_a(3))
+
+            def joined(self):
+                waited(inn.at[0], 0)
+                comb[0] = (p_wide[0] + inn[0].astype(F32)).astype(BF)
+                send(comb.at[0], from_l.at[:, first], ss.at[4], rs.at[4], at_a(1))
+                waited(inn.at[1], 1)
+                comb[1] = (p_wide[1] + inn[1].astype(F32)).astype(BF)
+                send(comb.at[1], from_r.at[:, second], ss.at[5], rs.at[5], at_a(3))
+
+            def mine(self):
+                group(0, own.at[:, first], own.at[:, second])
+
+            def across(self):
+                waited(from_l.at[:, second], 2)
+                waited(from_r.at[:, first], 3)
+                waited(from_l.at[:, first], 4)
+                waited(from_r.at[:, second], 5)
+                total(2, into_q(0))
+                send(q.at[0, :, first], qin.at[0], ss.at[6], rs.at[6], at_b(1))
+                send(q.at[0, :, second], qin.at[1], ss.at[7], rs.at[7], at_b(3))
+                total(1, into_q(1, 0))
+                send(q.at[1, :, second], ql.at[:, second], ss.at[8], rs.at[8], at_b(1))
+                total(3, into_q(2, 1))
+                send(q.at[2, :, first], qr.at[:, first], ss.at[9], rs.at[9], at_b(3))
+
+            def across_joined(self):
+                waited(qin.at[0], 6)
+                qcomb[0] = (q_wide[0] + qin[0].astype(F32)).astype(BF)
+                send(qcomb.at[0], ql.at[:, first], ss.at[10], rs.at[10], at_b(1))
+                waited(qin.at[1], 7)
+                qcomb[1] = (q_wide[1] + qin[1].astype(F32)).astype(BF)
+                send(qcomb.at[1], qr.at[:, second], ss.at[11], rs.at[11], at_b(3))
+
+            def result(self):
+                here = pl.ds(pl.multiple_of(pb * 48, 16), 48)
+                waited(ql.at[:, second], 8)
+                waited(qr.at[:, first], 9)
+                waited(ql.at[:, first], 10)
+                waited(qr.at[:, second], 11)
+                return (
+                    own[here, :]
+                    + from_l[here, :].astype(F32)
+                    + from_r[here, :].astype(F32)
+                    + ql[...].astype(F32)
+                    + qr[...].astype(F32)
+                )
+
+        return Stages()
 
     def small_sum(recv_ref, own_tile, ss, rs):
         acc = own_tile
@@ -318,10 +306,22 @@
 
     for i in range(1, 5):
         loads[i].wait()
-    proj = ring_sum(
-        scaled, wqkvo, N1, 256, a_p, a_own, a_in, a_comb, a_l, a_r, a_q, a_qin, a_qcomb, a_ql, a_qr,
-        ra_s, ra_r, gate_tiles,
-    )
+    qk = ring(0, *qk_bufs, qk_s, qk_r)
+    vo = ring(NH, *vo_bufs, vo_s, vo_r)
+    qk.opposite()
+    qk.plain()
+    vo.opposite()
+    gate_tiles()
+    qk.joined()
+    vo.plain()
+    vo.joined()
+    weight_send(0, 1, late, 2, at_a(1))
+    weight_send(0, 3, late, 3, at_a(3))
+    qk.mine()
+    vo.mine()
+    qk.across()
+    qk.across_joined()
+    vo.across()
     gsum = small_sum(grecv, gsend[kv], g_s, g_r)
     inv_row = lax.rsqrt(gsum[4:5, :] / D + EPS)
     inv_col = column_of(inv_row)[:48]
@@ -337,8 +337,9 @@
     w_own = column_of(jnp.exp(igate[0:1] - top))
     w_tail = jnp.exp(tail_log - top)
 
+    qk_sum = qk.result()
     for h in range(2):
-        qs[h] = proj(pl.ds(128 * h, 128)) * inv_col
+        qs[h] = qk_sum[:, 128 * h : 128 * h + 128] * inv_col
     for i in range(7, 10):
         loads[i].wait()
 
@@ -368,7 +369,9 @@
         sc_n[pl.ds(s, 1), :] = jnp.where(lane1 < 64, sc[0:1] + sc[1:2], sc[2:3] + sc[3:4])
         return 0
 
-    lax.fori_loop(0, 48, recall_step, 0, unroll=4)
+    lax.fori_loop(0, 24, recall_step, 0, unroll=4)
+    vo.across_joined()
+    lax.fori_loop(24, 48, recall_step, 0, unroll=4)
     sc_r = transpose_padded(sc_n[...])
     sc_t = jnp.where(lane64 < 64, sc_r[:64], pltpu.roll(sc_r[64:], 64, 1))
     weighted = w_tail * (sc_t * 128 ** (-0.5))
@@ -392,12 +395,13 @@
 
     tail_part = lax.fori_loop(0, 24, tail_step, jnp.zeros((128, 128), F32), unroll=4)
     w_state = column_of(w_inter)
+    vo_sum = vo.result()
     mixed = []
     for h in range(2):
         q = qs[h]
-        k = proj(pl.ds(256 + 128 * h, 128)) * inv_col * 128 ** (-0.5)
-        v = proj(pl.ds(512 + 128 * h, 128)) * inv_col
-        og = proj(pl.ds(768 + 128 * h, 128)) * inv_col
+        k = qk_sum[:, 256 + 128 * h : 384 + 128 * h] * inv_col * 128 ** (-0.5)
+        v = vo_sum[:, 128 * h : 128 * h + 128] * inv_col
+        og = vo_sum[:, 256 + 128 * h : 384 + 128 * h] * inv_col
         own = jnp.sum(q * k, axis=1, keepdims=True)
         rows = slice(64 * h, 64 * h + 48)
         recalled = mem_n[h] * w_state[rows] + tail_part[rows] + w_own[rows] * own * v
@@ -550,10 +554,6 @@
     b_wait(b_qin.at[1], 7)
     b_qcomb[1] = (b_own[b_rows(3), second] + b_qin[1].astype(F32)).astype(BF)
     send(b_qcomb.at[1], b_qr.at[:, second], rb_s.at[11], rb_r.at[11], left)
-    down_got(1, whole, 0)
-    down_send(1, 2, upper, 2, at_a(1))
-    down_got(3, whole, 1)
-    down_send(3, 2, lower, 3, at_a(3))
     for r in range(1, 8):
         src = mid_all.at[rows96(tp_from(r))]
         remote(src, src, mid_s.at[r], mid_r.at[r], (kv, tp)).wait_recv()
@@ -604,6 +604,10 @@
 
     hop(chunk(0), 0, at_b(1))
     hop(chunk(0), 1, at_b(3))
+    down_got(1, whole, 0)
+    down_send(1, 2, upper, 2, at_a(1))
+    down_got(3, whole, 1)
+    down_send(3, 2, lower, 3, at_a(3))
     arrived(chunk(1), 0)
     hop(chunk(1, (0, 32)), 2, at_b(1))
     arrived(chunk(3), 1)
@@ -688,6 +692,8 @@
             pltpu.VMEM((2, 48, n // 2), BF),
             pltpu.VMEM((48, n), BF),
             pltpu.VMEM((48, n), BF),
+            pltpu.VMEM((2, 192, n // 2), F32),
+            pltpu.VMEM((2, 48, n // 2), F32),
         ]
 
     scratch = [
@@ -707,7 +713,8 @@
         pltpu.VMEM((16, 8, 128), F32),
         pltpu.VMEM((8, 128), F32),
         pltpu.VMEM((128, 128), F32),
-        *ring_bufs(N1),
+        *ring_bufs(NH),
+        *ring_bufs(NH),
         pltpu.VMEM((2, 48, 128), F32),
         pltpu.VMEM((48, 8, 256), F32),
         pltpu.VMEM((2, 48, 128), F32),
@@ -722,7 +729,7 @@
         pltpu.VMEM((4, 192, 256), BF),
         pltpu.VMEM((2, 48, 256), BF),
         pltpu.VMEM((192, N2), F32),
-        *ring_bufs(N2)[6:],
+        *ring_bufs(N2)[6:11],
         pltpu.VMEM((192, FFD), BF),
         pltpu.VMEM((4, 8, 48, 128), BF),
         pltpu.VMEM((2, 4, 4, 48, 128), BF),
@@ -734,6 +741,7 @@
         dma((8,)), dma((8,)),
         dma((8,)), dma((8,)),
         dma((16,)), dma((16,)),
+        dma((12,)), dma((12,)),
         dma((12,)), dma((12,)),
         dma((12,)), dma((12,)),
         dma((6,)), dma((6,)),

time: 97.4 us -> 94.6 us (0.971)
  Pallas kernels: 95.8 us -> 93 us
    pallas_call x1, Pallas kernels: 95.8 us -> 93 us  [per_device(): pl.pallas_call(layer, out_shape=jax.ShapeDtypeStruct((32, 768), BF), in_s...]
where the time goes in v4:
time: 94.6 us; the launch traced here: 94.4 us
  Pallas kernels  93 us (98%)
  local copies, waits for them, and re-layouts  1.42 us (2%)
    pallas_call x1, Pallas kernels, per_device(): pl.pallas_call(layer, out_shape=jax.ShapeDtypeStruct((32, 768), BF), in_s...  93 us

profile of v4, /device:TPU:1, one launch (start us, length us, event | category | flops | bytes accessed | tf_op | source)
XLA Modules:
  0.0 94.4 jit_solution(17628689479126999218)
XLA Ops:
  0.0 93.0 %shard_map.208 = bf16[32,768]{1,0:T(8,128)(2,1)} custom-call(bf16[32,768]{1,0:T(8,128)(2,1)} %bitcast.13, f32[1,256]{1,0:T(1,128)} %bitcast.14, bf16[256,256]{1,0:T(8,128)(2,1)} %w_query.1, bf16[256,256]{1,0:T(8,128)(2,1)} %w_key.1, bf16[256,256]{1,0:T(8,128)(2,1)} %w_value.1, bf16[256,256]{1,0:T(8,128)(2,1)} %w_outgate.1, bf16[16,4096]{1,0:T(8,128)(2,1)} %bitcast.11, ...), custom_call_target="tpu_custom_call" | custom-call | tf_op jit(solution)/shard_map/pallas_call | solution.py:757
  93.0 1.4 %copy.24 = bf16[768,32]{0,1:T(8,128)(2,1)} copy(bf16[768,32]{0,1:T(8,128)(2,1)} %bitcast.10) | data formatting | bytes 98304

commit v5 on v4

--- a/solution.py
+++ b/solution.py
@@ -346,25 +346,21 @@
     for h in range(2):
         q_hi = qs[h].astype(BF).astype(F32)
         q_lo = (qs[h] - q_hi).astype(BF).astype(F32)
-        q_rows[:, 2 * h, :] = jnp.concatenate([q_hi, q_hi], axis=1)
-        q_rows[:, 2 * h + 1, :] = jnp.concatenate([q_lo, jnp.zeros((48, 128), F32)], axis=1)
+        q_rows[:, 2 * h, :] = q_hi
+        q_rows[:, 2 * h + 1, :] = q_lo
     for i in range(4, 8):
-        q_rows[:, i, :] = jnp.zeros((48, 256), F32)
+        q_rows[:, i, :] = jnp.zeros((48, 128), F32)
     contract_last = (((1,), (1,)), ((), ()))
     lane1 = lax.broadcasted_iota(jnp.int32, (1, 128), 1)
 
     def recall_step(s, _):
         lhs = q_rows[s].astype(BF)
-        state = cbuf[s].reshape(256, 128)
-        s_hi = state.astype(BF)
-        s_lo = (state - s_hi.astype(F32)).astype(BF)
-        m = lax.dot_general(
-            lhs, jnp.concatenate([s_hi, s_lo], axis=1), contract_last, preferred_element_type=F32
-        )
+        state = cbuf[s].reshape(256, 128).astype(BF)
+        m = lax.dot_general(lhs, state, contract_last, preferred_element_type=F32)
         mem_n[0, pl.ds(s, 1), :] = m[0:1, :128] + m[1:2, :128]
         mem_n[1, pl.ds(s, 1), :] = m[2:3, 128:] + m[3:4, 128:]
         sc = lax.dot_general(
-            lhs[:, :128], kbuf[s].reshape(128, 128), contract_last, preferred_element_type=F32
+            lhs, kbuf[s].reshape(128, 128), contract_last, preferred_element_type=F32
         )
         sc_n[pl.ds(s, 1), :] = jnp.where(lane1 < 64, sc[0:1] + sc[1:2], sc[2:3] + sc[3:4])
         return 0
@@ -380,18 +376,13 @@
     plane = lax.broadcasted_iota(jnp.int32, (128, 256), 1)
     slot = 2 * lax.rem(prow, 2) + lax.div(prow, 64)
     rows_w = jnp.where(lax.div(plane, 64) == slot, jnp.concatenate([rows_w, rows_w], axis=1), 0.0)
-    w_hi = rows_w.astype(BF)
-    w_lo = (rows_w - w_hi.astype(F32)).astype(BF)
+    rows_w = rows_w.astype(BF)
     step_of = lax.div(lax.rem(prow, 64), 2)
 
     def tail_step(g, acc):
         here = jnp.where(step_of == g, 1.0, 0.0).astype(BF)
         vals = vbuf[pl.ds(2 * g, 2)].reshape(256, 128)
-        return (
-            acc
-            + jnp.dot(w_hi * here, vals, preferred_element_type=F32)
-            + jnp.dot(w_lo * here, vals, preferred_element_type=F32)
-        )
+        return acc + jnp.dot(rows_w * here, vals, preferred_element_type=F32)
 
     tail_part = lax.fori_loop(0, 24, tail_step, jnp.zeros((128, 128), F32), unroll=4)
     w_state = column_of(w_inter)
@@ -414,16 +405,15 @@
         mine = mix_all.at[rows48(kv)]
         send(mine, mine, mix_s.at[i], mix_r.at[i], (kv_peer(i), tp))
     loads[10].wait()
-    for i in range(1, 16):
-        src = mix_all.at[rows48(kv_from(i))]
-        remote(src, src, mix_s.at[i], mix_r.at[i], (kv, tp)).wait_recv()
-
     weight_wait(1, early, 0)
     weight_wait(1, late, 2)
     weight_send(1, 2, (0, 128), 4, at_a(1))
     weight_wait(3, early, 1)
     weight_wait(3, late, 3)
     weight_send(3, 2, (128, 128), 5, at_a(3))
+    for i in (1, 3, 4, 12, 5, 7, 13, 15, 2, 8, 6, 9, 11, 14, 10):
+        src = mix_all.at[rows48(kv_from(i))]
+        remote(src, src, mix_s.at[i], mix_r.at[i], (kv, tp)).wait_recv()
     for r in [4, 3, 5, 2, 6, 1, 7, 0]:
         part = jnp.dot(mix_all[rows96(tp_peer(r)), :], wproj_v[...], preferred_element_type=F32)
         att_send[r] = part.astype(BF)
@@ -716,7 +706,7 @@
         *ring_bufs(NH),
         *ring_bufs(NH),
         pltpu.VMEM((2, 48, 128), F32),
-        pltpu.VMEM((48, 8, 256), F32),
+        pltpu.VMEM((48, 8, 128), F32),
         pltpu.VMEM((2, 48, 128), F32),
         pltpu.VMEM((48, 128), F32),
         pltpu.VMEM((768, 256), BF),

time: 94.6 us -> 93 us (0.983)
  Pallas kernels: 93 us -> 91.4 us
    pallas_call x1, Pallas kernels: 93 us -> 91.4 us  [per_device(): pl.pallas_call(layer, out_shape=jax.ShapeDtypeStruct((32, 768), BF), in_s...]
where the time goes in v5:
time: 93 us; the launch traced here: 92.8 us
  Pallas kernels  91.4 us (98%)
  local copies, waits for them, and re-layouts  1.42 us (2%)
    pallas_call x1, Pallas kernels, per_device(): pl.pallas_call(layer, out_shape=jax.ShapeDtypeStruct((32, 768), BF), in_s...  91.4 us

profile of v5, /device:TPU:1, one launch (start us, length us, event | category | flops | bytes accessed | tf_op | source)
XLA Modules:
  0.0 92.8 jit_solution(387453795413238473)
XLA Ops:
  0.0 91.4 %shard_map.208 = bf16[32,768]{1,0:T(8,128)(2,1)} custom-call(bf16[32,768]{1,0:T(8,128)(2,1)} %bitcast.13, f32[1,256]{1,0:T(1,128)} %bitcast.14, bf16[256,256]{1,0:T(8,128)(2,1)} %w_query.1, bf16[256,256]{1,0:T(8,128)(2,1)} %w_key.1, bf16[256,256]{1,0:T(8,128)(2,1)} %w_value.1, bf16[256,256]{1,0:T(8,128)(2,1)} %w_outgate.1, bf16[16,4096]{1,0:T(8,128)(2,1)} %bitcast.11, ...), custom_call_target="tpu_custom_call" | custom-call | tf_op jit(solution)/shard_map/pallas_call | solution.py:747
  91.4 1.4 %copy.24 = bf16[768,32]{0,1:T(8,128)(2,1)} copy(bf16[768,32]{0,1:T(8,128)(2,1)} %bitcast.10) | data formatting | bytes 98304
